TPU v7x, 32 devices: a whole 2x2x4 slice. The times are simulated.
32 devices in a mesh: kv: 8 (over z, y), tp: 4 (over x, core).
Axes of the slice: x: 2, y: 2, z: 4, core: 2. Of those that a mesh axis runs over, the one named last changes fastest.
Arguments:
- tokens: bfloat16 [5120, 4096], P('kv'), may hold values from -48 to 48
- query_weight: bfloat16 [4096, 2048], P(None, 'tp'), may hold values from -0.09375 to 0.09375
- key_weight: bfloat16 [4096, 512], P(None, 'tp'), may hold values from -0.09375 to 0.09375
- value_weight: bfloat16 [4096, 512], P(None, 'tp'), may hold values from -0.09375 to 0.09375
- gate_weight: bfloat16 [4096, 64], replicated, may hold values from -0.09375 to 0.09375
- summary_pos: bfloat16 [32, 64], replicated, may hold values from -6 to 6
- key_mixing: bfloat16 [32, 8], replicated, may hold values from -1 to 1
- value_mixing: bfloat16 [32, 8], replicated, may hold values from -1 to 1
- out_weight: bfloat16 [2048, 4096], P('tp'), may hold values from -0.125 to 0.125
- chosen: int32 [80, 8, 16], P('kv', 'tp'), may hold values from 0 to 79, as said below
Outputs:
- mixed: bfloat16 [5120, 4096], P(('kv', 'tp'))
Inputs may be any that keep to these rules, and one draw needn't show every extreme that they name: `chosen`: entry [b, g, 0] is b itself; every entry is at most b. For the query blocks of one index of kv, one key head and any OTHER index of kv, at most 2 distinct blocks of that index's 64-position blocks are named, and exactly 2 of the index just before. Entries may repeat.
All inputs are finite; a program needn't handle non-finite values.
Results may differ from a plain program's by a relative error of at most 0.013.
The roundings to bfloat16 on the way count: a program that leaves them out, or rounds other values in their place, can miss the bound.
Values may be sent and summed in bfloat16 or wider, within the bound.
A program may use at most 192 MiB of HBM per device.

v0:
```python
import functools

import jax
import jax.numpy as jnp
from jax import lax
from jax.experimental import pallas as pl
from jax.experimental.pallas import tpu as pltpu
from jax.sharding import PartitionSpec as P

HD = 64
CMP = 32
SB = 64
N_SEL = 16
LANES = 128
LOW = -1e30
F32 = jnp.float32
BF16 = jnp.bfloat16
MESH = pl.DeviceIdType.MESH
VMEM_LIMIT = 64_000_000


def project(
    n, G, R, nb, kc, pad, ow_load, idx_smem, sem_idx,
    tok_hbm, qw_hbm, kw_hbm, vw_hbm, gw_hbm, ch_ref, km_ref, vm_ref, pos_in,
    qp_ref, gate_ref, tab_ref, sum_ref, idx_ref, bias_ref,
    tok, qw, kvw, gw, acc, gacc, tf, named, pos_ref, req_ref, req_in, req_smem, sem_req, send, sum_send,
    sem_tok, sem_kw, sem_vw, sem_qw, sem_gw,
    req_s, req_r, blk_s, blk_r, sum_s, sum_r,
):
    tp = lax.axis_index("tp")
    me = lax.axis_index("kv")
    rows = nb * SB
    depth = tok.shape[1]
    chunks = depth // kc
    spans = rows // CMP
    kvd = G * HD

    def part(i):
        return pl.ds(i * kc, kc)

    def loads(i):
        return [
            pltpu.make_async_copy(tok_hbm.at[:, part(i)], tok.at[:, part(i)], sem_tok.at[i]),
            pltpu.make_async_copy(kw_hbm.at[part(i)], kvw.at[part(i), pl.ds(0, kvd)], sem_kw.at[i]),
            pltpu.make_async_copy(vw_hbm.at[part(i)], kvw.at[part(i), pl.ds(kvd, kvd)], sem_vw.at[i]),
        ]

    def late(i):
        return [
            pltpu.make_async_copy(qw_hbm.at[part(i)], qw.at[part(i)], sem_qw.at[i]),
            pltpu.make_async_copy(gw_hbm.at[:, part(i)], gw.at[:, part(i)], sem_gw.at[i]),
        ]

    for i in range(chunks):
        for c in loads(i):
            c.start()

    barrier = pltpu.get_barrier_semaphore()
    for i in range(1, n):
        pl.semaphore_signal(
            barrier, inc=1, device_id={"kv": lax.rem(me + i, n)}, device_id_type=MESH
        )
    for i in range(1, 4):
        pl.semaphore_signal(barrier, inc=1, device_id={"tp": lax.rem(tp + i, 4)}, device_id_type=MESH)

    place = lax.broadcasted_iota(jnp.int32, named.shape, 1)
    slot_row = lax.broadcasted_iota(jnp.int32, (LANES, N_SEL * SB), 0)
    slot_col = lax.broadcasted_iota(jnp.int32, (LANES, N_SEL * SB), 1) // SB
    spread = jnp.where(slot_row == slot_col, 1.0, 0.0).astype(BF16)
    for g in range(G):
        named[...] = jnp.full(named.shape, -1, jnp.int32)
        named[:nb, :N_SEL] = ch_ref[:, g, :]
        c = named[...]
        source = jnp.zeros_like(c)
        for s in range(1, n):
            source = source + jnp.where(c >= s * nb, 1, 0)
        inside = c - source * nb
        low_of = jnp.zeros_like(c)
        for s in range(n):
            hit = (c >= 0) & (source == s)
            lo = jnp.where(hit, inside, nb)
            lo = jnp.min(jnp.min(lo, axis=0, keepdims=True), axis=1, keepdims=True)
            lo = jnp.where(lo == nb, 0, lo)
            hi = jnp.where(hit, inside, 0)
            hi = jnp.max(jnp.max(hi, axis=0, keepdims=True), axis=1, keepdims=True)
            low_of = jnp.where(hit, lo, low_of)
            req_ref[s, 2 * g : 2 * g + 1] = jnp.broadcast_to(lo, (1, LANES))
            req_ref[s, 2 * g + 1 : 2 * g + 2] = jnp.broadcast_to(hi, (1, LANES))
        away = G * nb + (source * G + g) * 2 + jnp.where(inside != low_of, 1, 0)
        at = jnp.where(source == me, g * nb + inside, away)
        idx_ref[g] = jnp.where(c >= 0, at, 0)
        again = jnp.zeros(c.shape, F32)
        for d in range(1, N_SEL):
            again = jnp.where((place >= d) & (pltpu.roll(c, d, 1) == c), 1.0, again)
        bias_ref[g] = jnp.dot(again.astype(BF16), spread, preferred_element_type=F32) * LOW

    idx_copy = pltpu.make_async_copy(idx_ref, idx_smem, sem_idx)
    idx_copy.start()
    pl.semaphore_wait(barrier, n + 2)

    def req_copy(i):
        return pltpu.make_async_remote_copy(
            src_ref=req_ref.at[lax.rem(me + n - i, n)], dst_ref=req_in.at[i],
            send_sem=req_s.at[i], recv_sem=req_r.at[i],
            device_id={"kv": lax.rem(me + n - i, n)}, device_id_type=MESH,
        )

    def blk_copy(i):
        return pltpu.make_async_remote_copy(
            src_ref=send.at[i],
            dst_ref=tab_ref.at[pl.ds(G * nb + me * G * 2, G * 2)],
            send_sem=blk_s.at[i], recv_sem=blk_r.at[i],
            device_id={"kv": lax.rem(me + i, n)}, device_id_type=MESH,
        )

    def blk_arrival(i):
        s = lax.rem(me + n - i, n)
        return pltpu.make_async_remote_copy(
            src_ref=send.at[i],
            dst_ref=tab_ref.at[pl.ds(G * nb + s * G * 2, G * 2)],
            send_sem=blk_s.at[i], recv_sem=blk_r.at[i],
            device_id={"kv": lax.rem(me + i, n)}, device_id_type=MESH,
        )

    def sum_copy(i):
        return pltpu.make_async_remote_copy(
            src_ref=sum_send, dst_ref=sum_ref.at[me],
            send_sem=sum_s.at[i], recv_sem=sum_r.at[i],
            device_id={"kv": lax.rem(me + i, n)}, device_id_type=MESH,
        )

    def sum_arrival(i):
        return pltpu.make_async_remote_copy(
            src_ref=sum_send, dst_ref=sum_ref.at[lax.rem(me + n - i, n)],
            send_sem=sum_s.at[i], recv_sem=sum_r.at[i],
            device_id={"kv": lax.rem(me + i, n)}, device_id_type=MESH,
        )

    for i in range(1, n):
        req_copy(i).start()

    acc[:, : 2 * kvd] = jnp.zeros((rows, 2 * kvd), F32)

    def kv_step(i, carry):
        for c in loads(i):
            c.wait()
        for c in late(i):
            c.start()
        acc[:, : 2 * kvd] += jnp.dot(tok[:, part(i)], kvw[part(i), :], preferred_element_type=F32)
        return carry

    lax.fori_loop(0, chunks, kv_step, 0)
    ow_load.start()
    lane = lax.broadcasted_iota(jnp.int32, (SB, LANES), 1)
    lower = lane < HD

    def table_step(b, carry):
        r0 = pl.ds(b * SB, SB)
        for pair in range(G // 2):
            keys = acc[r0, pair * LANES : (pair + 1) * LANES].astype(BF16).astype(F32)
            vals = acc[r0, kvd + pair * LANES : kvd + (pair + 1) * LANES].astype(BF16).astype(F32)
            first = jnp.where(lower, keys, pltpu.roll(vals, HD, 1))
            second = jnp.where(lower, pltpu.roll(keys, HD, 1), vals)
            for g, t in ((2 * pair, first), (2 * pair + 1, second)):
                tf[g * nb + b] = t.astype(BF16)
                tab_ref[g * nb + b] = t.astype(BF16)
        return carry

    lax.fori_loop(0, nb, table_step, 0)
    pos_ref[:, :HD] = pos_in[...].astype(F32)
    pos_ref[:, HD:] = pos_in[...].astype(F32)
    mix_row = lax.broadcasted_iota(jnp.int32, km_ref.shape, 0)
    mix_low = lax.broadcasted_iota(jnp.int32, (CMP, LANES), 1) < HD
    diagonal = lax.broadcasted_iota(jnp.int32, (CMP, CMP), 0) == lax.broadcasted_iota(
        jnp.int32, (CMP, CMP), 1
    )

    def mix_column(ref, head):
        line = jnp.where(mix_row == head, ref[...].astype(F32), 0.0)
        line = jnp.sum(line, axis=0, keepdims=True)
        return jnp.sum(jnp.where(diagonal, line, 0.0), axis=1, keepdims=True)

    for g in range(G):
        head = lax.axis_index("tp") * G + g
        km = mix_column(km_ref, head)
        vm = mix_column(vm_ref, head)
        mix = jnp.where(mix_low, km, vm)
        t = tf[g * nb : (g + 1) * nb].astype(F32).reshape(spans, CMP, LANES)
        w = (t + pos_ref[...][None]) * mix[None]
        s = jnp.sum(w, axis=1)
        s = jnp.concatenate([s, jnp.zeros((pad - spans, LANES), F32)], axis=0)
        sum_send[g] = s.astype(BF16)
        sum_ref[me, g] = s.astype(BF16)
    for i in range(1, n):
        sum_copy(i).start()
    for i in range(1, n):
        req_copy(i).wait_recv()
        pltpu.make_async_copy(req_in.at[i], req_smem.at[i], sem_req.at[i]).start()
    for i in range(1, n):
        pltpu.make_async_copy(req_in.at[i], req_smem.at[i], sem_req.at[i]).wait()

        @pl.when(me + i < n)
        def _():
            for k in range(G * 2):
                send[i, k] = tf[(k // 2) * nb + req_smem[i, k, 0]]
            blk_copy(i).start()

    acc[...] = jnp.zeros_like(acc)
    gacc[...] = jnp.zeros_like(gacc)

    def q_step(i, carry):
        for c in late(i):
            c.wait()
        acc[...] += jnp.dot(tok[:, part(i)], qw[part(i), :], preferred_element_type=F32)
        gacc[...] += lax.dot_general(
            tok[:, part(i)], gw[:, part(i)], (((1,), (1,)), ((), ())), preferred_element_type=F32
        )
        return carry

    lax.fori_loop(0, chunks, q_step, 0)
    gate_ref[...] = jax.nn.sigmoid(gacc[...])

    def query_step(b, carry):
        r0 = pl.ds(b * SB, SB)
        for g in range(G):
            for pair in range(R // 2):
                at = (g * R // 2 + pair) * LANES
                t = acc[r0, at : at + LANES].astype(BF16).astype(F32) * (HD ** -0.5)
                even = jnp.where(lower, t, 0.0)
                odd = jnp.where(lower, pltpu.roll(t, HD, 1), 0.0)
                qp_ref[g, b, 2 * pair * SB : (2 * pair + 1) * SB, :] = even.astype(BF16)
                qp_ref[g, b, (2 * pair + 1) * SB : (2 * pair + 2) * SB, :] = odd.astype(BF16)
        return carry

    lax.fori_loop(0, nb, query_step, 0)
    idx_copy.wait()
    for i in range(1, n):
        sum_arrival(i).wait_recv()
        sum_copy(i).wait_send()
        req_copy(i).wait_send()

        @pl.when(me + i < n)
        def _():
            blk_copy(i).wait_send()

        @pl.when(me - i >= 0)
        def _():
            blk_arrival(i).wait_recv()


def attend_and_mix(
    n, G, R, nb, pad, spans, cw, load,
    idx_ref, qp_ref, gate_ref, tab_ref, sum_ref, bias_ref,
    out_ref,
    ow, att, kbuf, mine, dsend, drecv, early, esend, erecv, xsend, xrecv, base,
    d_s, d_r, e_s, e_r, x_s, x_r,
):
    me = lax.axis_index("kv")
    tp = lax.axis_index("tp")
    core = lax.rem(tp, 2)
    side = tp // 2
    partner = side * 2 + 1 - core
    rows = nb * SB
    quarter = rows // 4
    half_blocks = nb // 2
    width = out_ref.shape[1]
    chunks = width // cw
    group_rows = R * SB
    side_cols = width // 2
    step_rows = SB // 2

    row = lax.broadcasted_iota(jnp.int32, (group_rows, LANES), 0) % SB
    lane = lax.broadcasted_iota(jnp.int32, (group_rows, LANES), 1)
    tri = jnp.where((lane < SB) & (lane > row), LOW, 0.0)
    span_lane = lax.broadcasted_iota(jnp.int32, (group_rows, n * pad), 1)
    span_in = span_lane % pad
    span_end = ((span_lane // pad) * spans + span_in) * CMP + (CMP - 1)
    span_row = lax.broadcasted_iota(jnp.int32, (group_rows, n * pad), 0) % SB
    low64 = lax.broadcasted_iota(jnp.int32, (SB, LANES), 1) < HD
    gate_lane = lax.broadcasted_iota(jnp.int32, (SB, gate_ref.shape[1]), 1)
    nt = (((1,), (1,)), ((), ()))

    def attend(b, carry):
        gates = gate_ref[pl.ds(b * SB, SB), :]
        seen = (span_in < spans) & (span_end - span_row <= me * rows + b * SB)
        for g in range(G):
            for j in range(N_SEL):
                kbuf[g, j * SB : (j + 1) * SB, :] = tab_ref[idx_ref[g, b, j]]
            kb = kbuf[g]
            q = qp_ref[g, b]
            s = lax.dot_general(q, kb, nt, preferred_element_type=F32)
            s = s + bias_ref[g, pl.ds(b, 1), :]
            s = jnp.concatenate([s[:, :LANES] + tri, s[:, LANES:]], axis=1)
            m = jnp.max(s, axis=-1, keepdims=True)
            p = jnp.exp(s - m)
            l = jnp.sum(p, axis=-1, keepdims=True)
            oc = jnp.dot(p.astype(BF16), kb, preferred_element_type=F32)
            sm = sum_ref[:, g].reshape(n * pad, LANES)
            s2 = lax.dot_general(q, sm, nt, preferred_element_type=F32)
            s2 = jnp.where(seen, s2, LOW)
            m2 = jnp.max(s2, axis=-1, keepdims=True)
            p2 = jnp.where(seen, jnp.exp(s2 - m2), 0.0)
            l2 = jnp.sum(p2, axis=-1, keepdims=True)
            os = jnp.dot(p2.astype(BF16), sm, preferred_element_type=F32)
            ic = 1.0 / l
            i2 = jnp.where(l2 > 0.0, 1.0 / jnp.where(l2 > 0.0, l2, 1.0), 0.0)
            parts = []
            for r in range(R):
                at = (tp * G * R + g * R + r) * 2
                g0 = jnp.sum(jnp.where(gate_lane == at, gates, 0.0), axis=-1, keepdims=True)
                g1 = jnp.sum(jnp.where(gate_lane == at + 1, gates, 0.0), axis=-1, keepdims=True)
                k = slice(r * SB, (r + 1) * SB)
                parts.append(os[k] * (g0 * i2[k]) + oc[k] * (g1 * ic[k]))
            for pair in range(R // 2):
                t = jnp.where(low64, pltpu.roll(parts[2 * pair], HD, 1), parts[2 * pair + 1])
                at = (g * R // 2 + pair) * LANES
                att[pl.ds(b * SB, SB), at : at + LANES] = t.astype(BF16)
        return carry

    def d_copy(j):
        return pltpu.make_async_remote_copy(
            src_ref=dsend.at[j], dst_ref=drecv.at[j],
            send_sem=d_s.at[j], recv_sem=d_r.at[j],
            device_id={"tp": partner}, device_id_type=MESH,
        )

    def e_copy(i):
        return pltpu.make_async_remote_copy(
            src_ref=esend.at[i], dst_ref=erecv.at[i],
            send_sem=e_s.at[i], recv_sem=e_r.at[i],
            device_id={"tp": partner}, device_id_type=MESH,
        )

    def x_copy(k):
        step = lax.rem(k, half_blocks)
        return pltpu.make_async_remote_copy(
            src_ref=xsend.at[k], dst_ref=xrecv.at[core, step],
            send_sem=x_s.at[k], recv_sem=x_r.at[core, step],
            device_id={"tp": (1 - side) * 2 + k // half_blocks}, device_id_type=MESH,
        )

    def x_arrival(c, step):
        return pltpu.make_async_remote_copy(
            src_ref=xsend.at[step], dst_ref=xrecv.at[c, step],
            send_sem=x_s.at[step], recv_sem=x_r.at[c, step],
            device_id={"tp": (1 - side) * 2 + core}, device_id_type=MESH,
        )

    other_first = (1 - side) * half_blocks

    def early_block(i):
        attend(other_first + i, 0)
        a = att[pl.ds((other_first + i) * SB, SB), :]
        for j in range(side_cols // cw):
            cols = pl.ds(pl.multiple_of((1 - core) * side_cols + j * cw, cw), cw)
            esend[i, :, j * cw : (j + 1) * cw] = jnp.dot(
                a, ow[:, cols], preferred_element_type=F32
            ).astype(BF16)
        e_copy(i).start()
        for j in range(side_cols // cw):
            cols = pl.ds(pl.multiple_of(core * side_cols + j * cw, cw), cw)
            early[i, :, j * cw : (j + 1) * cw] = jnp.dot(
                a, ow[:, cols], preferred_element_type=F32
            ).astype(BF16)

    def forward(i):
        e_copy(i).wait_recv()
        for k in range(2):
            r = slice(k * step_rows, (k + 1) * step_rows)
            xsend[2 * i + k] = (early[i, r].astype(F32) + erecv[i, r].astype(F32)).astype(BF16)
            x_copy(2 * i + k).start()

    load.wait()

    def early_step(i, carry):
        early_block(i)
        forward(i)
        return carry

    lax.fori_loop(0, half_blocks, early_step, 0)

    own_first = side * half_blocks
    lax.fori_loop(own_first, own_first + half_blocks, attend, 0)

    def own_step(j, carry):
        w = ow[:, pl.ds(pl.multiple_of(j * cw, cw), cw)]
        theirs = att[pl.ds(own_first * SB + (1 - core) * quarter, quarter), :]
        dsend[j] = jnp.dot(theirs, w, preferred_element_type=F32).astype(BF16)
        d_copy(j).start()
        ours = att[pl.ds(own_first * SB + core * quarter, quarter), :]
        mine[j] = jnp.dot(ours, w, preferred_element_type=F32).astype(BF16)
        return carry

    lax.fori_loop(0, chunks, own_step, 0)

    def base_step(j, carry):
        d_copy(j).wait_recv()
        cols = pl.ds(pl.multiple_of(j * cw, cw), cw)
        base[:, cols] = mine[j].astype(F32) + drecv[j].astype(F32)
        d_copy(j).wait_send()
        return carry

    lax.fori_loop(0, chunks, base_step, 0)

    def last_step(k, carry):
        r = pl.ds(pl.multiple_of(k * step_rows, step_rows), step_rows)
        for c in range(2):
            x_arrival(c, k).wait_recv()
            cols = slice(c * side_cols, (c + 1) * side_cols)
            out_ref[r, cols] = (base[r, cols] + xrecv[c, k].astype(F32)).astype(BF16)
        e_copy(k).wait_send()
        x_copy(k).wait_send()
        x_copy(half_blocks + k).wait_send()
        return carry

    lax.fori_loop(0, half_blocks, last_step, 0)


def layer_kernel(n, G, R, nb, kc, pad, cw, *refs):
    inputs, ow_hbm, out_ref = refs[:9], refs[9], refs[10]
    qp, gate, tab, summary, idx, bias = refs[11:17]
    idx_smem, sem_idx, ow, sem_w = refs[17:21]
    first, second = refs[21 : 21 + 26], refs[21 + 26 :]
    load = pltpu.make_async_copy(ow_hbm, ow, sem_w)
    project(
        n, G, R, nb, kc, pad, load, idx_smem, sem_idx,
        *inputs, qp, gate, tab, summary, idx, bias, *first,
    )
    attend_and_mix(
        n, G, R, nb, pad, nb * SB // CMP, cw, load,
        idx_smem, qp, gate, tab, summary, bias, out_ref, ow, *second,
    )


def local(
    n,
    tokens, query_weight, key_weight, value_weight, gate_weight,
    summary_pos, key_mixing, value_mixing, out_weight, chosen,
):
    rows, depth = tokens.shape
    heads = query_weight.shape[1] // HD
    G = key_weight.shape[1] // HD
    R = heads // G
    nb = rows // SB
    spans = rows // CMP
    pad = -(-spans // 16) * 16
    kc = min(1024, depth)
    chunks = depth // kc
    width = out_weight.shape[1]
    cw = 512
    oc = width // cw
    gates_all = gate_weight.shape[1]

    vmem = pl.BlockSpec(memory_space=pltpu.VMEM)
    hbm = pl.BlockSpec(memory_space=pl.ANY)
    dma = pltpu.SemaphoreType.DMA
    table = G * nb + n * G * 2
    nbp = -(-nb // 8) * 8
    quarter = rows // 4
    half = nb // 2
    stage_one = [
        pltpu.VMEM((rows, depth), BF16),
        pltpu.VMEM((depth, heads * HD), BF16),
        pltpu.VMEM((depth, 2 * G * HD), BF16),
        pltpu.VMEM((gates_all, depth), BF16),
        pltpu.VMEM((rows, heads * HD), F32),
        pltpu.VMEM((rows, gates_all), F32),
        pltpu.VMEM((G * nb, SB, LANES), BF16),
        pltpu.VMEM((nbp, LANES), jnp.int32),
        pltpu.VMEM((CMP, LANES), F32),
        pltpu.VMEM((n, 8, LANES), jnp.int32),
        pltpu.VMEM((n, 8, LANES), jnp.int32),
        pltpu.SMEM((n, 8, LANES), jnp.int32),
        dma((n,)),
        pltpu.VMEM((n, G * 2, SB, LANES), BF16),
        pltpu.VMEM((G, pad, LANES), BF16),
        dma((chunks,)), dma((chunks,)), dma((chunks,)), dma((chunks,)), dma((chunks,)),
        dma((n,)), dma((n,)), dma((n,)), dma((n,)), dma((n,)), dma((n,)),
    ]
    stage_two = [
        pltpu.VMEM((rows, heads * HD), BF16),
        pltpu.VMEM((G, N_SEL * SB, LANES), BF16),
        pltpu.VMEM((oc, quarter, cw), BF16),
        pltpu.VMEM((oc, quarter, cw), BF16),
        pltpu.VMEM((oc, quarter, cw), BF16),
        pltpu.VMEM((half, SB, width // 2), BF16),
        pltpu.VMEM((half, SB, width // 2), BF16),
        pltpu.VMEM((half, SB, width // 2), BF16),
        pltpu.VMEM((2 * half, SB // 2, width // 2), BF16),
        pltpu.VMEM((2, half, SB // 2, width // 2), BF16),
        pltpu.VMEM((quarter, width), F32),
        dma((oc,)), dma((oc,)), dma((half,)), dma((half,)), dma((2 * half,)), dma((2, half)),
    ]
    return pl.pallas_call(
        functools.partial(layer_kernel, n, G, R, nb, kc, pad, cw),
        name="layer",
        out_shape=jax.ShapeDtypeStruct((quarter, width), BF16),
        in_specs=[hbm] * 5 + [vmem] * 4 + [hbm],
        out_specs=vmem,
        scratch_shapes=[
            pltpu.VMEM((G, nb, R * SB, LANES), BF16),
            pltpu.VMEM((rows, gates_all), F32),
            pltpu.VMEM((table, SB, LANES), BF16),
            pltpu.VMEM((n, G, pad, LANES), BF16),
            pltpu.VMEM((G, nbp, LANES), jnp.int32),
            pltpu.VMEM((G, nbp, N_SEL * SB), F32),
            pltpu.SMEM((G, nbp, LANES), jnp.int32),
            dma,
            pltpu.VMEM(out_weight.shape, BF16),
            dma,
            *stage_one,
            *stage_two,
        ],
        compiler_params=pltpu.CompilerParams(
            collective_id=1, has_side_effects=True, vmem_limit_bytes=VMEM_LIMIT
        ),
    )(
        tokens, query_weight, key_weight, value_weight, gate_weight.T,
        chosen, key_mixing.T, value_mixing.T, summary_pos, out_weight,
    )


def solution(mesh):
    placed = (
        P("kv", None),
        P(None, "tp"),
        P(None, "tp"),
        P(None, "tp"),
        P(),
        P(),
        P(),
        P(),
        P("tp", None),
        P("kv", "tp", None),
    )
    return jax.shard_map(
        functools.partial(local, mesh.shape["kv"]),
        mesh=mesh, in_specs=placed, out_specs=P(("kv", "tp"), None), check_vma=False,
    )
```

profile of v0, /device:TPU:29, one launch (start us, length us, event | category | flops | bytes accessed | tf_op | source)
XLA Modules:
  0.0 60.6 jit_solution(3101881251818012941)
XLA Ops:
  0.0 58.1 %layer.1 = bf16[160,4096]{1,0:T(8,128)(2,1)} custom-call(bf16[640,4096]{1,0:T(8,128)(2,1)} %refs_0_.1, bf16[4096,512]{1,0:T(8,128)(2,1)} %refs_1_.1, bf16[4096,128]{1,0:T(8,128)(2,1)} %refs_2_.1, bf16[4096,128]{1,0:T(8,128)(2,1)} %refs_3_.1, bf16[64,4096]{1,0:T(8,128)(2,1)} %bitcast.3, s32[10,2,16]{2,1,0:T(2,128)} %refs_5_.1, bf16[8,32]{1,0:T(8,128)(2,1)} %bitcast.4, ...), custom_call_target="tpu_custom_call" | custom-call | tf_op jit(solution)/shard_map/layer/pallas_call | solution.py:494
  58.1 2.5 %copy.12 = bf16[160,4096]{1,0:T(8,128)(2,1)} copy(bf16[160,4096]{1,0:T(8,128)(2,1)} %layer.1) | data formatting | bytes 2621440
where the time goes:
time: 60.9 us; the launch traced here: 60.6 us
  Pallas kernels  58.1 us (95%)
  local copies, waits for them, and re-layouts  2.49 us (4%)
    pallas_call x1, Pallas kernels, local(): pl.pallas_call(functools.partial(layer_kernel, n, G, R, nb, kc, pad, cw),...  58.1 us
    unnamed x1, local copies, waits for them, and re-layouts  2.49 us

commit v1 on v0

v1 whole, which is shorter than its diff:
```python
import functools
import types

import jax
import jax.numpy as jnp
from jax import lax
from jax.experimental import pallas as pl
from jax.experimental.pallas import tpu as pltpu
from jax.sharding import PartitionSpec as P

HD = 64
CMP = 32
SB = 64
N_SEL = 16
LANES = 128
PIECES = 4
LOW = -1e30
F32 = jnp.float32
BF16 = jnp.bfloat16
MESH = pl.DeviceIdType.MESH
VMEM_LIMIT = 64_000_000
NT = (((1,), (1,)), ((), ()))


def requests(n, G, nb, k):
    place = lax.broadcasted_iota(jnp.int32, k.named.shape, 1)
    for g in range(G):
        k.named[g] = jnp.full(k.named.shape[1:], -1, jnp.int32)
        k.named[g, :nb, :N_SEL] = k.chosen[:, g, :]
        c = k.named[g]
        source = jnp.zeros_like(c)
        for s in range(1, n):
            source = source + jnp.where(c >= s * nb, 1, 0)
        inside = c - source * nb
        for s in range(n):
            hit = (c >= 0) & (source == s)
            lo = jnp.where(hit, inside, nb)
            lo = jnp.min(jnp.min(lo, axis=0, keepdims=True), axis=1, keepdims=True)
            lo = jnp.where(lo == nb, 0, lo)
            hi = jnp.where(hit, inside, 0)
            hi = jnp.max(jnp.max(hi, axis=0, keepdims=True), axis=1, keepdims=True)
            k.req[s, 2 * g : 2 * g + 1] = jnp.broadcast_to(lo, (1, LANES))
            k.req[s, 2 * g + 1 : 2 * g + 2] = jnp.broadcast_to(hi, (1, LANES))


def biases(n, G, nb, k, me):
    for g in range(G):
        c = k.named[g]
        lane = lax.broadcasted_iota(jnp.int32, c.shape, 1)
        bias = jnp.full(c.shape, LOW, F32)

        def mark(bias, hit, at):
            hit = jnp.max(jnp.where(hit, 1.0, 0.0), axis=1, keepdims=True)
            return jnp.where((lane == at) & (hit > 0.0), 0.0, bias)

        for j in range(nb):
            bias = mark(bias, c == me * nb + j, j)
        for s in range(n - 1):
            lo = k.req[s, 2 * g : 2 * g + 1]
            hi = k.req[s, 2 * g + 1 : 2 * g + 2]
            at = jnp.where(me > s, nb + 2 * (me - s - 1), -5)
            real = c >= 0
            bias = mark(bias, real & (c == s * nb + lo), at)
            bias = mark(bias, real & (c == s * nb + hi) & (hi != lo), at + 1)
        k.bias[g] = bias


class Travel:
    def __init__(self, k, pieces):
        tp, me = lax.axis_index("tp"), lax.axis_index("kv")
        core, side = lax.rem(tp, 2), tp // 2
        self.k, self.pieces = k, pieces
        self.across = {"tp": (1 - side) * 2 + core}
        self.partner = {"tp": side * 2 + 1 - core}
        self.beside = {"kv": me + 1 - 2 * lax.rem(me, 2)}
        self.mine = lax.rem(me, 2)
        self.columns = k.wfar.shape[2]
        self.first = k.ow.shape[1] - self.columns
        self.size = self.columns // 2 // pieces

    def cols(self, half, j, base=0):
        at = base + half * (self.columns // 2) + j * self.size
        return pl.ds(pl.multiple_of(at, LANES), self.size)

    def copy(self, src, dst, send, recv, target):
        return pltpu.make_async_remote_copy(
            src_ref=src, dst_ref=dst, send_sem=send, recv_sem=recv,
            device_id=target, device_id_type=MESH,
        )

    def x(self, j):
        k = self.k
        return self.copy(
            k.ow_hbm.at[:, self.cols(self.mine, j, self.first)], k.wfar.at[1, :, self.cols(self.mine, j)],
            k.wx_s.at[j], k.wx_r.at[j], self.across,
        )

    def p(self):
        k = self.k
        return self.copy(
            k.ow_hbm.at[:, pl.ds(self.first, self.columns)], k.wfar.at[0], k.wp_s, k.wp_r, self.partner
        )

    def y(self, j):
        here = self.k.wfar.at[1, :, self.cols(self.mine, j)]
        return self.copy(here, here, self.k.wy_s.at[j], self.k.wy_r.at[j], self.beside)

    def y_arrival(self, j):
        here = self.k.wfar.at[1, :, self.cols(1 - self.mine, j)]
        return self.copy(here, here, self.k.wy_s.at[j], self.k.wy_r.at[j], self.beside)

    def d(self, h, j):
        k = self.k
        at = self.cols(self.mine if h == 0 else 1 - self.mine, j)
        return self.copy(
            k.wfar.at[1, :, at], k.wfar.at[2, :, at], k.wd_s.at[h, j], k.wd_r.at[h, j], self.partner
        )

    def start(self):
        for j in range(self.pieces):
            self.x(j).start()
        self.p().start()

    def relay_x(self, j):
        self.x(j).wait_recv()
        self.y(j).start()
        self.d(0, j).start()

    def relay_y(self, j):
        self.y_arrival(j).wait_recv()
        self.d(1, j).start()

    def arrived(self):
        self.p().wait_recv()
        for h in range(2):
            for j in range(self.pieces):
                self.d(h, j).wait_recv()

    def sent(self):
        self.p().wait_send()
        for j in range(self.pieces):
            self.x(j).wait_send()
            self.y(j).wait_send()
            for h in range(2):
                self.d(h, j).wait_send()


def project(n, G, R, nb, kc, k, ow_loads, travel):
    tp = lax.axis_index("tp")
    me = lax.axis_index("kv")
    rows = nb * SB
    depth = k.tok.shape[1]
    chunks = depth // kc
    spans = rows // CMP
    slot = k.sum_send.shape[0] // 2

    def part(i):
        return pl.ds(i * kc, kc)

    def loads(i):
        return [
            pltpu.make_async_copy(k.tok_hbm.at[:, part(i)], k.tok.at[:, part(i)], k.sem_tok.at[i]),
            pltpu.make_async_copy(k.kw_hbm.at[part(i)], k.kvw.at[part(i), pl.ds(0, LANES)], k.sem_kw.at[i]),
            pltpu.make_async_copy(k.vw_hbm.at[part(i)], k.kvw.at[part(i), pl.ds(LANES, LANES)], k.sem_vw.at[i]),
        ]

    half_gates = k.gw.shape[0] // 2

    def late(i):
        return [
            pltpu.make_async_copy(k.qw_hbm.at[part(i)], k.qw.at[part(i)], k.sem_qw.at[i]),
            pltpu.make_async_copy(k.gw_hbm.at[:, part(i)], k.gw.at[pl.ds(0, half_gates), part(i)], k.sem_gw.at[0, i]),
            pltpu.make_async_copy(k.gw_hbm.at[:, part(i)], k.gw.at[pl.ds(half_gates, half_gates), part(i)], k.sem_gw.at[1, i]),
        ]

    for i in range(chunks):
        for c in loads(i):
            c.start()

    barrier = pltpu.get_barrier_semaphore()
    for i in range(1, n):
        pl.semaphore_signal(
            barrier, inc=1, device_id={"kv": lax.rem(me + i, n)}, device_id_type=MESH
        )
    for i in range(1, 4):
        pl.semaphore_signal(barrier, inc=1, device_id={"tp": lax.rem(tp + i, 4)}, device_id_type=MESH)

    requests(n, G, nb, k)
    pl.semaphore_wait(barrier, n + 2)

    def req_copy(i):
        return pltpu.make_async_remote_copy(
            src_ref=k.req.at[lax.rem(me + n - i, n)], dst_ref=k.req_in.at[i],
            send_sem=k.req_s.at[i], recv_sem=k.req_r.at[i],
            device_id={"kv": lax.rem(me + n - i, n)}, device_id_type=MESH,
        )

    def req_local(i):
        return pltpu.make_async_copy(k.req_in.at[i], k.req_smem.at[i], k.sem_req.at[i])

    def blk_copy(i):
        return pltpu.make_async_remote_copy(
            src_ref=k.send.at[i], dst_ref=k.far.at[i - 1],
            send_sem=k.blk_s.at[i], recv_sem=k.blk_r.at[i],
            device_id={"kv": lax.rem(me + i, n)}, device_id_type=MESH,
        )

    def sum_copy(i):
        return pltpu.make_async_remote_copy(
            src_ref=k.sum_send, dst_ref=k.sum_in.at[i],
            send_sem=k.sum_s.at[i], recv_sem=k.sum_r.at[i],
            device_id={"kv": lax.rem(me + i, n)}, device_id_type=MESH,
        )

    for i in range(1, n):
        req_copy(i).start()
    travel.start()

    biases(n, G, nb, k, me)
    bias_copy = pltpu.make_async_copy(k.bias, k.bias_smem, k.sem_bias)
    bias_copy.start()
    for i in range(1, n):

        @pl.when(me < i)
        def _():
            k.far[i - 1] = jnp.zeros(k.far.shape[1:], BF16)

    k.sum_key[...] = jnp.zeros_like(k.sum_key)
    k.sum_val[...] = jnp.zeros_like(k.sum_val)
    k.acc[:, : 2 * LANES] = jnp.zeros((rows, 2 * LANES), F32)

    def kv_step(i, carry):
        for c in loads(i):
            c.wait()
        for c in late(i):
            c.start()
        k.acc[:, : 2 * LANES] += jnp.dot(k.tok[:, part(i)], k.kvw[part(i), :], preferred_element_type=F32)
        return carry

    lax.fori_loop(0, chunks, kv_step, 0)
    first = range(1, min(4, n))
    for i in first:
        req_copy(i).wait_recv()
        req_local(i).start()
    for c in ow_loads:
        c.start()
    low = lax.broadcasted_iota(jnp.int32, (SB, LANES), 1) < HD
    mix_row = lax.broadcasted_iota(jnp.int32, k.km.shape, 0)
    mix_low = lax.broadcasted_iota(jnp.int32, (CMP, LANES), 1) < HD
    diagonal = lax.broadcasted_iota(jnp.int32, (CMP, CMP), 0) == lax.broadcasted_iota(
        jnp.int32, (CMP, CMP), 1
    )

    def mix_column(ref, head):
        line = jnp.where(mix_row == head, ref[...].astype(F32), 0.0)
        line = jnp.sum(line, axis=0, keepdims=True)
        return jnp.sum(jnp.where(diagonal, line, 0.0), axis=1, keepdims=True)

    k.pos_wide[:, :HD] = k.pos[...].astype(F32)
    k.pos_wide[:, HD:] = k.pos[...].astype(F32)
    both = []
    for ref, at in ((k.km, 0), (k.vm, LANES)):
        mix = jnp.where(mix_low, mix_column(ref, tp * G), mix_column(ref, tp * G + 1))
        t = k.acc[:, at : at + LANES].astype(BF16).astype(F32).reshape(spans, CMP, LANES)
        s = jnp.sum((t + k.pos_wide[...][None]) * mix[None], axis=1)
        both.append(jnp.concatenate([s, jnp.zeros((slot - spans, LANES), F32)], axis=0))
    both = jnp.concatenate(both, axis=0).astype(BF16)
    k.sum_send[...] = both
    k.sum_key[:slot] = both.astype(F32)[:slot]
    k.sum_val[:slot] = both.astype(F32)[slot:]
    for i in range(1, n):

        @pl.when(me + i < n)
        def _():
            sum_copy(i).start()

    for t in range(nb // 2):
        r0 = slice(t * LANES, (t + 1) * LANES)
        keys = k.acc[r0, :LANES].astype(BF16).astype(F32)
        vals = jnp.transpose(k.acc[r0, LANES : 2 * LANES].astype(BF16).astype(F32))
        k.keys[r0, :] = keys.astype(BF16)
        k.vals[:, r0] = vals.astype(BF16)
        keys_r = pltpu.roll(keys, HD, 1)
        vals_r = pltpu.roll(vals, HD, 1)
        for h in range(2):
            kk, kr = keys[h * SB : (h + 1) * SB], keys_r[h * SB : (h + 1) * SB]
            v_left, v_right = (vals, vals_r) if h == 0 else (vals_r, vals)
            for g in range(G):
                left, right = (kk, kr) if g == 0 else (kr, kk)
                v = slice(g * HD, (g + 1) * HD)
                c = g * nb + 2 * t + h
                k.left[c, :SB] = jnp.where(low, left, 0.0).astype(BF16)
                k.left[c, SB:] = jnp.where(low, v_left[v], 0.0).astype(BF16)
                k.right[c, :SB] = jnp.where(low, 0.0, right).astype(BF16)
                k.right[c, SB:] = jnp.where(low, 0.0, v_right[v]).astype(BF16)
    def answer(i):
        req_local(i).wait()

        @pl.when(me + i < n)
        def _():
            for g in range(G):
                lo = k.req_smem[i, 2 * g, 0]
                hi = k.req_smem[i, 2 * g + 1, 0]
                k.send[i, g] = k.left[g * nb + lo] + k.right[g * nb + hi]
            blk_copy(i).start()

    for i in reversed(first):
        answer(i)
    for i in range(len(first) + 1, n):
        req_copy(i).wait_recv()
        req_local(i).start()
    for i in range(n - 1, len(first), -1):
        answer(i)

    k.acc[...] = jnp.zeros_like(k.acc)
    k.gacc[...] = jnp.zeros_like(k.gacc)

    def q_step(i, carry):
        for c in late(i):
            c.wait()
        k.acc[...] += jnp.dot(k.tok[:, part(i)], k.qw[part(i), :], preferred_element_type=F32)
        k.gacc[...] += lax.dot_general(
            k.tok[:, part(i)], k.gw[:, part(i)], NT, preferred_element_type=F32
        )
        return carry

    lax.fori_loop(0, chunks, q_step, 0)
    travel.relay_x(0)
    wide_low = lax.broadcasted_iota(jnp.int32, k.gacc.shape, 1) < half_gates
    gates = jax.nn.sigmoid(k.gacc[...])
    gates_hi = gates.astype(BF16).astype(F32)
    gates = jnp.where(wide_low, gates_hi, gates - gates_hi).astype(BF16)
    spread_row = lax.broadcasted_iota(jnp.int32, (LANES, G * R * HD), 0)
    spread_col = lax.broadcasted_iota(jnp.int32, (LANES, G * R * HD), 1)
    spread_at = (tp * G * R + spread_col // HD) * 2
    for branch in range(2):
        spread = jnp.where(spread_row % half_gates == spread_at + branch, 1.0, 0.0).astype(BF16)
        k.gate[branch] = jnp.dot(gates, spread, preferred_element_type=F32)

    def query_step(b, carry):
        r0 = pl.ds(b * SB, SB)
        for g in range(G):
            for pair in range(R // 2):
                at = (g * R // 2 + pair) * LANES
                t = k.acc[r0, at : at + LANES].astype(BF16).astype(F32) * (HD ** -0.5)
                turned = pltpu.roll(t, HD, 1)
                e = 2 * pair * SB
                o = e + SB
                k.q[g, b, e : e + SB] = jnp.where(low, t, 0.0).astype(BF16)
                k.q[g, b, o : o + SB] = jnp.where(low, turned, 0.0).astype(BF16)
                k.q[g, b, R * SB + e : R * SB + e + SB] = jnp.where(low, 0.0, turned).astype(BF16)
                k.q[g, b, R * SB + o : R * SB + o + SB] = jnp.where(low, 0.0, t).astype(BF16)
        return carry

    lax.fori_loop(0, nb, query_step, 0)
    bias_copy.wait()
    for i in range(1, n):
        req_copy(i).wait_send()

        @pl.when(me + i < n)
        def _():
            sum_copy(i).wait_send()

        @pl.when(me - i >= 0)
        def _():
            sum_copy(i).wait_recv()
            both = k.sum_in[i].astype(F32)
            k.sum_key[i * slot : (i + 1) * slot] = both[:slot]
            k.sum_val[i * slot : (i + 1) * slot] = both[slot:]

    k.sum_keys[...] = k.sum_key[...].astype(BF16)
    k.sum_vals[...] = jnp.transpose(k.sum_val[...]).astype(BF16)
    span = lax.broadcasted_iota(jnp.int32, k.until.shape, 0)
    row = lax.broadcasted_iota(jnp.int32, k.until.shape, 1) % SB
    source, t = span // slot, span % slot
    k.until[...] = jnp.where(
        (t < spans) & (source <= me) & (source < n),
        (t - spans * source) * CMP + (CMP - 1) - row, 1 << 30,
    )

    def blocks_done():
        for i in range(1, n):

            @pl.when(me + i < n)
            def _():
                blk_copy(i).wait_send()

            @pl.when(me - i >= 0)
            def _():
                blk_copy(i).wait_recv()

    return blocks_done


def row8(x):
    return jnp.max(x.reshape(x.shape[0] // 8, 8, x.shape[1]), axis=0)


def sum8(x):
    return jnp.sum(x.reshape(x.shape[0] // 8, 8, x.shape[1]), axis=0)


def turn(outs):
    t = jnp.transpose(jnp.concatenate(outs, axis=0))
    turned = pltpu.roll(t, HD, 1)
    low = lax.broadcasted_iota(jnp.int32, (SB, LANES), 1) < HD
    tiles = []
    for first, second in ((t, turned), (turned, t)):
        for e in range(0, t.shape[0], 2 * SB):
            tiles.append(jnp.where(low, first[e : e + SB], second[e + SB : e + 2 * SB]))
    return tiles


def near(n, G, R, nb, k, blocks, b, carry):
    width = R * SB
    q = jnp.concatenate([k.q[g, b, g * width : (g + 1) * width] for g in range(G)], axis=0)
    keys = blocks * SB
    k.score[:keys] = lax.dot_general(k.keys[:keys], q, NT, preferred_element_type=F32)
    own = pl.ds(b * SB, SB)
    shape = (SB, G * width)
    later = lax.broadcasted_iota(jnp.int32, shape, 0) > lax.broadcasted_iota(jnp.int32, shape, 1) % SB
    k.score[own, :] += jnp.where(later, LOW, 0.0)

    def bias(j):
        return jnp.concatenate([jnp.full((8, width), k.bias_smem[g, b, j], F32) for g in range(G)], axis=1)

    top = None
    for j in range(blocks):
        t = row8(k.score[j * SB : (j + 1) * SB]) + bias(j)
        top = t if top is None else jnp.maximum(top, t)
    top = jnp.max(top, axis=0, keepdims=True)
    total = jnp.zeros((8, G * width), F32)
    weights = []
    for j in range(blocks):
        p = jnp.exp(k.score[j * SB : (j + 1) * SB] - (top - bias(j)[:1]))
        total = total + sum8(p)
        weights.append(p.astype(BF16))
    weights = jnp.concatenate(weights, axis=0)
    k.top[b] = jnp.broadcast_to(top, k.top.shape[1:])
    k.total[b] = total
    for g in range(G):
        cols = slice(g * width, (g + 1) * width)
        k.part[b, :, cols] = jnp.dot(
            k.vals[g * HD : (g + 1) * HD, :keys], weights[:, cols], preferred_element_type=F32
        )

    s = lax.dot_general(k.sum_keys[...], q, NT, preferred_element_type=F32)
    until = jnp.concatenate([k.until[...]] * (G * width // LANES), axis=1)
    s = jnp.where(until <= b * SB, s, LOW)
    top = jnp.max(row8(s), axis=0, keepdims=True)
    p = jnp.exp(s - top)
    total = jnp.sum(sum8(p), axis=0, keepdims=True)
    scale = jnp.where(top > LOW * 0.5, 1.0 / total, 0.0)
    p = p.astype(BF16)
    outs = []
    for g in range(G):
        cols = slice(g * width, (g + 1) * width)
        o = jnp.dot(k.sum_vals[g * HD : (g + 1) * HD, :], p[:, cols], preferred_element_type=F32)
        outs.append(o * scale[:, cols])
    for t, tile in enumerate(turn(outs)):
        cols = slice(t * LANES, (t + 1) * LANES)
        k.mixed[own, cols] = tile * k.gate[0, own, cols]
    return carry


def distant(n, G, R, nb, k, b):
    width = R * SB
    own = pl.ds(b * SB, SB)
    outs = []
    for g in range(G):
        cols = slice(g * width, (g + 1) * width)
        keys = k.far[:, g, :SB, :].reshape((n - 1) * SB, LANES)
        k.far_score[g] = lax.dot_general(keys, k.q[g, b], NT, preferred_element_type=F32)

        def bias(i, h):
            return k.bias_smem[g, b, nb + 2 * i + h]

        before = k.top[b, :1, cols]
        top = jnp.broadcast_to(before, (8, width))
        for i in range(n - 1):
            t = row8(k.far_score[g, i * SB : (i + 1) * SB])
            for h in range(2):
                top = jnp.maximum(top, t[:, h * width : (h + 1) * width] + bias(i, h))
        top = jnp.max(top, axis=0, keepdims=True)
        keep = jnp.exp(before - top)
        total = k.total[b, :, cols] * keep
        weights = []
        for i in range(n - 1):
            for h in range(2):
                s = k.far_score[g, i * SB : (i + 1) * SB, h * width : (h + 1) * width]
                p = jnp.exp(s - (top - bias(i, h)))
                total = total + sum8(p)
                weights.append(p.astype(BF16))
        weights = jnp.concatenate(weights, axis=0)
        vals = jnp.concatenate([k.far[i, g, SB:, :] for i in range(n - 1)], axis=1)
        o = k.part[b, :, cols] * keep + jnp.dot(vals, weights, preferred_element_type=F32)
        outs.append(o * (1.0 / jnp.sum(total, axis=0, keepdims=True)))
    for t, tile in enumerate(turn(outs)):
        cols = slice(t * LANES, (t + 1) * LANES)
        k.att[own, cols] = (k.mixed[own, cols] + tile * k.gate[1, own, cols]).astype(BF16)


def attend_and_mix(n, G, R, nb, cw, k, ow_loads, blocks_done, travel):
    tp = lax.axis_index("tp")
    core = lax.rem(tp, 2)
    side = tp // 2
    partner = side * 2 + 1 - core
    rows = nb * SB
    quarter = rows // 4
    half_blocks = nb // 2
    width = k.base.shape[1]
    chunks = width // cw
    side_cols = width // 2
    step_rows = SB // 2
    att, ow = k.att, k.ow

    few = (nb // 2 + 1) // 2 * 2

    def near_blocks(which):
        @pl.when(which == 0)
        def _():
            lax.fori_loop(0, half_blocks, functools.partial(near, n, G, R, nb, k, few), 0)

        @pl.when(which == 1)
        def _():
            lax.fori_loop(half_blocks, nb, functools.partial(near, n, G, R, nb, k, nb), 0)

    near_blocks(1 - side)
    for c in ow_loads:
        c.wait()
    travel.relay_x(1)
    blocks_done()

    def d_copy(j):
        return pltpu.make_async_remote_copy(
            src_ref=k.dsend.at[j], dst_ref=k.drecv.at[j],
            send_sem=k.d_s.at[j], recv_sem=k.d_r.at[j],
            device_id={"tp": partner}, device_id_type=MESH,
        )

    def e_copy(i):
        return pltpu.make_async_remote_copy(
            src_ref=k.esend.at[i], dst_ref=k.erecv.at[i],
            send_sem=k.e_s.at[i], recv_sem=k.e_r.at[i],
            device_id={"tp": partner}, device_id_type=MESH,
        )

    def x_copy(i):
        step = lax.rem(i, half_blocks)
        return pltpu.make_async_remote_copy(
            src_ref=k.xsend.at[i], dst_ref=k.xrecv.at[core, step],
            send_sem=k.x_s.at[i], recv_sem=k.x_r.at[core, step],
            device_id={"tp": (1 - side) * 2 + i // half_blocks}, device_id_type=MESH,
        )

    def x_arrival(c, step):
        return pltpu.make_async_remote_copy(
            src_ref=k.xsend.at[step], dst_ref=k.xrecv.at[c, step],
            send_sem=k.x_s.at[step], recv_sem=k.x_r.at[c, step],
            device_id={"tp": (1 - side) * 2 + core}, device_id_type=MESH,
        )

    other_first = (1 - side) * half_blocks

    def a_copy(i):
        to, step = i // half_blocks, lax.rem(i, half_blocks)
        rows_of = pl.ds(pl.multiple_of(other_first * SB + i * step_rows, step_rows), step_rows)
        into = pl.ds(pl.multiple_of(step * step_rows, step_rows), step_rows)
        return pltpu.make_async_remote_copy(
            src_ref=att.at[rows_of], dst_ref=k.att_in.at[1 + lax.rem(to + core, 2), into],
            send_sem=k.a_s.at[i], recv_sem=k.a_r.at[core, step],
            device_id={"tp": (1 - side) * 2 + to}, device_id_type=MESH,
        )

    def a_arrival(c, step):
        into = pl.ds(pl.multiple_of(step * step_rows, step_rows), step_rows)
        return pltpu.make_async_remote_copy(
            src_ref=att.at[into], dst_ref=k.att_in.at[1 + lax.rem(c + core, 2), into],
            send_sem=k.a_s.at[step], recv_sem=k.a_r.at[c, step],
            device_id={"tp": (1 - side) * 2 + core}, device_id_type=MESH,
        )

    def early_block(i):
        distant(n, G, R, nb, k, other_first + i)
        for h in range(2):
            a_copy(2 * i + h).start()
        a = att[pl.ds((other_first + i) * SB, SB), :]
        for j in range(side_cols // cw):
            cols = pl.ds(pl.multiple_of((1 - core) * side_cols + j * cw, cw), cw)
            k.esend[i, :, j * cw : (j + 1) * cw] = jnp.dot(
                a, ow[:, cols], preferred_element_type=F32
            ).astype(BF16)
        e_copy(i).start()
        for j in range(side_cols // cw):
            cols = pl.ds(pl.multiple_of(core * side_cols + j * cw, cw), cw)
            k.early[i, :, j * cw : (j + 1) * cw] = jnp.dot(
                a, ow[:, cols], preferred_element_type=F32
            ).astype(BF16)

    def forward(i):
        e_copy(i).wait_recv()
        for h in range(2):
            r = slice(h * step_rows, (h + 1) * step_rows)
            k.xsend[2 * i + h] = (k.early[i, r].astype(F32) + k.erecv[i, r].astype(F32)).astype(BF16)
            x_copy(2 * i + h).start()

    def early_step(i, carry):
        early_block(i)
        forward(i)
        for at, relay, j in ((0, travel.relay_x, 2), (1, travel.relay_y, 0), (2, travel.relay_x, 3), (3, travel.relay_y, 1)):

            @pl.when(i == min(at, half_blocks - 1))
            def _():
                relay(j)

        return carry

    lax.fori_loop(0, half_blocks, early_step, 0)

    own_first = side * half_blocks
    near_blocks(side)

    def own_att(b, carry):
        distant(n, G, R, nb, k, b)
        return carry

    lax.fori_loop(own_first, own_first + half_blocks, own_att, 0)
    theirs_at = pl.ds(pl.multiple_of(own_first * SB + (1 - core) * quarter, step_rows), quarter)
    ours_at = pl.ds(pl.multiple_of(own_first * SB + core * quarter, step_rows), quarter)
    p_copy = pltpu.make_async_remote_copy(
        src_ref=att.at[theirs_at], dst_ref=k.att_in.at[0], send_sem=k.p_s, recv_sem=k.p_r,
        device_id={"tp": partner}, device_id_type=MESH,
    )
    p_copy.start()
    travel.relay_y(2)

    def own_step(j, carry):
        w = ow[:, pl.ds(pl.multiple_of(j * cw, cw), cw)]
        theirs = att[theirs_at, :]
        k.dsend[j] = jnp.dot(theirs, w, preferred_element_type=F32).astype(BF16)
        d_copy(j).start()
        ours = att[ours_at, :]
        k.mine[j] = jnp.dot(ours, w, preferred_element_type=F32).astype(BF16)
        return carry

    lax.fori_loop(0, chunks, own_step, 0)

    travel.relay_y(3)
    travel.arrived()
    p_copy.wait_recv()
    for c in range(2):
        for step in range(half_blocks):
            a_arrival(c, step).wait_recv()

    def wide_step(j, carry):
        cols = pl.ds(pl.multiple_of(j * cw, cw), cw)
        out_cols = pl.ds(pl.multiple_of(travel.first + j * cw, cw), cw)
        o = jnp.dot(att[ours_at, :], ow[:, out_cols], preferred_element_type=F32)
        for slot in range(3):
            o = o + jnp.dot(k.att_in[slot], k.wfar[slot, :, cols], preferred_element_type=F32)
        k.out[:, out_cols] = o.astype(BF16)
        return carry

    lax.fori_loop(0, travel.columns // cw, wide_step, 0)
    def base_step(j, carry):
        d_copy(j).wait_recv()
        cols = pl.ds(pl.multiple_of(j * cw, cw), cw)
        k.base[:, cols] = k.mine[j].astype(F32) + k.drecv[j].astype(F32)
        d_copy(j).wait_send()
        return carry

    lax.fori_loop(0, chunks, base_step, 0)

    def last_step(s, carry):
        r = pl.ds(pl.multiple_of(s * step_rows, step_rows), step_rows)
        for c in range(2):
            x_arrival(c, s).wait_recv()
            cols = slice(c * side_cols, (c + 1) * side_cols)
            k.out[r, cols] = (k.base[r, cols] + k.xrecv[c, s].astype(F32)).astype(BF16)
        e_copy(s).wait_send()
        x_copy(s).wait_send()
        x_copy(half_blocks + s).wait_send()
        a_copy(s).wait_send()
        a_copy(half_blocks + s).wait_send()
        return carry

    lax.fori_loop(0, half_blocks, last_step, 0)
    p_copy.wait_send()
    travel.sent()


def layer_kernel(n, G, R, nb, kc, cw, names, *refs):
    k = types.SimpleNamespace(**dict(zip(names, refs, strict=True)))
    ow_loads = [pltpu.make_async_copy(k.ow_hbm, k.ow, k.sem_ow)]
    travel = Travel(k, PIECES)
    blocks_done = project(n, G, R, nb, kc, k, ow_loads, travel)
    attend_and_mix(n, G, R, nb, cw, k, ow_loads, blocks_done, travel)


def local(
    n,
    tokens, query_weight, key_weight, value_weight, gate_weight,
    summary_pos, key_mixing, value_mixing, out_weight, chosen,
):
    rows, depth = tokens.shape
    heads = query_weight.shape[1] // HD
    G = key_weight.shape[1] // HD
    R = heads // G
    nb = rows // SB
    spans = rows // CMP
    slot = -(-spans // 8) * 8
    all_spans = -(-n * slot // LANES) * LANES
    kc = min(1024, depth)
    chunks = depth // kc
    width = out_weight.shape[1]
    cw = 512
    wide = width // 2
    summed = width - wide
    oc = summed // cw
    gates_all = gate_weight.shape[1]
    assert G == 2 and n % 2 == 0 and 2 * gates_all == LANES and nb % 2 == 0

    vmem = pl.BlockSpec(memory_space=pltpu.VMEM)
    hbm = pl.BlockSpec(memory_space=pl.ANY)
    dma = pltpu.SemaphoreType.DMA
    V = pltpu.VMEM
    nbp = -(-nb // 8) * 8
    quarter = rows // 4
    half = nb // 2
    inputs = ["tok_hbm", "qw_hbm", "kw_hbm", "vw_hbm", "gw_hbm", "chosen", "km", "vm", "pos", "ow_hbm"]
    scratch = {
        "q": V((G, nb, 2 * R * SB, LANES), BF16),
        "tok": V((rows, depth), BF16),
        "qw": V((depth, heads * HD), BF16),
        "kvw": V((depth, 2 * LANES), BF16),
        "gw": V((LANES, depth), BF16),
        "ow": V(out_weight.shape, BF16),
        "acc": V((rows, heads * HD), F32),
        "gacc": V((rows, LANES), F32),
        "gate": V((2, rows, heads * HD), F32),
        "keys": V((rows, LANES), BF16),
        "vals": V((LANES, rows), BF16),
        "left": V((G * nb, 2 * SB, LANES), BF16),
        "right": V((G * nb, 2 * SB, LANES), BF16),
        "named": V((G, nbp, LANES), jnp.int32),
        "bias": V((G, nbp, LANES), F32),
        "bias_smem": pltpu.SMEM((G, nbp, LANES), F32),
        "pos_wide": V((CMP, LANES), F32),
        "req": V((n, 8, LANES), jnp.int32),
        "req_in": V((n, 8, LANES), jnp.int32),
        "req_smem": pltpu.SMEM((n, 8, LANES), jnp.int32),
        "send": V((n, G, 2 * SB, LANES), BF16),
        "far": V((n - 1, G, 2 * SB, LANES), BF16),
        "sum_send": V((2 * slot, LANES), BF16),
        "sum_in": V((n, 2 * slot, LANES), BF16),
        "sum_key": V((all_spans, LANES), F32),
        "sum_val": V((all_spans, LANES), F32),
        "sum_keys": V((all_spans, LANES), BF16),
        "sum_vals": V((LANES, all_spans), BF16),
        "until": V((all_spans, LANES), jnp.int32),
        "score": V((rows, heads * HD), F32),
        "far_score": V((G, (n - 1) * SB, 2 * R * SB), F32),
        "top": V((nb, 8, heads * HD), F32),
        "total": V((nb, 8, heads * HD), F32),
        "part": V((nb, HD, heads * HD), F32),
        "mixed": V((rows, heads * HD), F32),
        "att": V((rows, heads * HD), BF16),
        "mine": V((oc, quarter, cw), BF16),
        "dsend": V((oc, quarter, cw), BF16),
        "drecv": V((oc, quarter, cw), BF16),
        "early": V((half, SB, summed // 2), BF16),
        "esend": V((half, SB, summed // 2), BF16),
        "erecv": V((half, SB, summed // 2), BF16),
        "xsend": V((2 * half, SB // 2, summed // 2), BF16),
        "xrecv": V((2, half, SB // 2, summed // 2), BF16),
        "base": V((quarter, summed), F32),
        "wfar": V((3, out_weight.shape[0], wide), BF16),
        "att_in": V((3, quarter, heads * HD), BF16),
        "sem_ow": dma,
        "sem_bias": dma,
        "sem_req": dma((n,)),
        "sem_tok": dma((chunks,)), "sem_kw": dma((chunks,)), "sem_vw": dma((chunks,)),
        "sem_qw": dma((chunks,)), "sem_gw": dma((2, chunks)),
        "req_s": dma((n,)), "req_r": dma((n,)), "blk_s": dma((n,)), "blk_r": dma((n,)),
        "sum_s": dma((n,)), "sum_r": dma((n,)),
        "d_s": dma((oc,)), "d_r": dma((oc,)), "e_s": dma((half,)), "e_r": dma((half,)),
        "x_s": dma((2 * half,)), "x_r": dma((2, half)),
        "a_s": dma((2 * half,)), "a_r": dma((2, half)), "p_s": dma, "p_r": dma,
        "wx_s": dma((PIECES,)), "wx_r": dma((PIECES,)), "wp_s": dma, "wp_r": dma,
        "wy_s": dma((PIECES,)), "wy_r": dma((PIECES,)),
        "wd_s": dma((2, PIECES)), "wd_r": dma((2, PIECES)),
    }
    return pl.pallas_call(
        functools.partial(layer_kernel, n, G, R, nb, kc, cw, inputs + ["out"] + list(scratch)),
        name="layer",
        out_shape=pltpu.VMEM((quarter, width), BF16),
        in_specs=[hbm] * 5 + [vmem] * 4 + [hbm],
        out_specs=vmem,
        scratch_shapes=list(scratch.values()),
        compiler_params=pltpu.CompilerParams(
            collective_id=1, has_side_effects=True, vmem_limit_bytes=VMEM_LIMIT
        ),
    )(
        tokens, query_weight, key_weight, value_weight, gate_weight.T,
        chosen, key_mixing.T, value_mixing.T, summary_pos, out_weight,
    )


def solution(mesh):
    placed = (
        P("kv", None),
        P(None, "tp"),
        P(None, "tp"),
        P(None, "tp"),
        P(),
        P(),
        P(),
        P(),
        P("tp", None),
        P("kv", "tp", None),
    )
    return jax.shard_map(
        functools.partial(local, mesh.shape["kv"]),
        mesh=mesh, in_specs=placed, out_specs=P(("kv", "tp"), None), check_vma=False,
    )
```

time: 60.9 us -> 57.5 us (0.944)
  the two profiles are of different devices: /device:TPU:29 before, /device:TPU:1 now
where the time goes in v1:
time: 57.5 us; the launch traced here: 57.3 us
  Pallas kernels  56.2 us (98%)
  local copies, waits for them, and re-layouts  1.06 us (2%)
    pallas_call x1, Pallas kernels, local(): pl.pallas_call(functools.partial(layer_kernel, n, G, R, nb, kc, cw, input...  56.2 us

profile of v1, /device:TPU:1, one launch (start us, length us, event | category | flops | bytes accessed | tf_op | source)
XLA Modules:
  0.0 57.3 jit_solution(123175271492344565)
XLA Ops:
  0.0 56.2 %layer.1 = bf16[160,4096]{1,0:T(8,128)(2,1)S(1)} custom-call(bf16[640,4096]{1,0:T(8,128)(2,1)} %refs_0_.1, bf16[4096,512]{1,0:T(8,128)(2,1)} %refs_1_.1, bf16[4096,128]{1,0:T(8,128)(2,1)} %refs_2_.1, bf16[4096,128]{1,0:T(8,128)(2,1)} %refs_3_.1, bf16[64,4096]{1,0:T(8,128)(2,1)} %bitcast.3, s32[10,2,16]{2,1,0:T(2,128)} %refs_5_.1, bf16[8,32]{1,0:T(8,128)(2,1)} %bitcast.4, ...), custom_call_target="tpu_custom_call" | custom-call | tf_op jit(solution)/shard_map/layer/pallas_call | solution.py:793
  56.2 1.1 %copy.12 = bf16[160,4096]{1,0:T(8,128)(2,1)} copy(bf16[160,4096]{1,0:T(8,128)(2,1)S(1)} %layer.1) | data formatting | bytes 2621440

commit v2 on v1

--- a/solution.py
+++ b/solution.py
@@ -225,6 +225,8 @@
         def _():
             k.far[i - 1] = jnp.zeros(k.far.shape[1:], BF16)
 
+    k.q_near[...] = jnp.zeros_like(k.q_near)
+    k.q_far[...] = jnp.zeros_like(k.q_far)
     k.sum_key[...] = jnp.zeros_like(k.sum_key)
     k.sum_val[...] = jnp.zeros_like(k.sum_val)
     k.acc[:, : 2 * LANES] = jnp.zeros((rows, 2 * LANES), F32)
@@ -238,10 +240,6 @@
         return carry
 
     lax.fori_loop(0, chunks, kv_step, 0)
-    first = range(1, min(4, n))
-    for i in first:
-        req_copy(i).wait_recv()
-        req_local(i).start()
     for c in ow_loads:
         c.start()
     low = lax.broadcasted_iota(jnp.int32, (SB, LANES), 1) < HD
@@ -259,11 +257,13 @@
     k.pos_wide[:, :HD] = k.pos[...].astype(F32)
     k.pos_wide[:, HD:] = k.pos[...].astype(F32)
     both = []
-    for ref, at in ((k.km, 0), (k.vm, LANES)):
+    for ref, at, more in ((k.km, 0, 1.0), (k.vm, LANES, 0.0)):
         mix = jnp.where(mix_low, mix_column(ref, tp * G), mix_column(ref, tp * G + 1))
         t = k.acc[:, at : at + LANES].astype(BF16).astype(F32).reshape(spans, CMP, LANES)
         s = jnp.sum((t + k.pos_wide[...][None]) * mix[None], axis=1)
-        both.append(jnp.concatenate([s, jnp.zeros((slot - spans, LANES), F32)], axis=0))
+        if slot > spans:
+            s = jnp.concatenate([s, s[: slot - spans] * more], axis=0)
+        both.append(s)
     both = jnp.concatenate(both, axis=0).astype(BF16)
     k.sum_send[...] = both
     k.sum_key[:slot] = both.astype(F32)[:slot]
@@ -293,6 +293,10 @@
                 k.left[c, SB:] = jnp.where(low, v_left[v], 0.0).astype(BF16)
                 k.right[c, :SB] = jnp.where(low, 0.0, right).astype(BF16)
                 k.right[c, SB:] = jnp.where(low, 0.0, v_right[v]).astype(BF16)
+    first = range(1, min(4, n))
+    for i in first:
+        req_copy(i).wait_recv()
+        req_local(i).start()
     def answer(i):
         req_local(i).wait()
 
@@ -306,12 +310,6 @@
 
     for i in reversed(first):
         answer(i)
-    for i in range(len(first) + 1, n):
-        req_copy(i).wait_recv()
-        req_local(i).start()
-    for i in range(n - 1, len(first), -1):
-        answer(i)
-
     k.acc[...] = jnp.zeros_like(k.acc)
     k.gacc[...] = jnp.zeros_like(k.gacc)
 
@@ -324,7 +322,13 @@
         )
         return carry
 
-    lax.fori_loop(0, chunks, q_step, 0)
+    q_step(0, 0)
+    for i in range(len(first) + 1, n):
+        req_copy(i).wait_recv()
+        req_local(i).start()
+    for i in range(n - 1, len(first), -1):
+        answer(i)
+    lax.fori_loop(1, chunks, q_step, 0)
     travel.relay_x(0)
     wide_low = lax.broadcasted_iota(jnp.int32, k.gacc.shape, 1) < half_gates
     gates = jax.nn.sigmoid(k.gacc[...])
@@ -337,22 +341,25 @@
         spread = jnp.where(spread_row % half_gates == spread_at + branch, 1.0, 0.0).astype(BF16)
         k.gate[branch] = jnp.dot(gates, spread, preferred_element_type=F32)
 
-    def query_step(b, carry):
-        r0 = pl.ds(b * SB, SB)
+    tall_low = lax.broadcasted_iota(jnp.int32, (HD, LANES), 1) < SB
+
+    def query_step(t, carry):
+        r0 = pl.ds(pl.multiple_of(t * LANES, LANES), LANES)
         for g in range(G):
             for pair in range(R // 2):
                 at = (g * R // 2 + pair) * LANES
-                t = k.acc[r0, at : at + LANES].astype(BF16).astype(F32) * (HD ** -0.5)
-                turned = pltpu.roll(t, HD, 1)
-                e = 2 * pair * SB
-                o = e + SB
-                k.q[g, b, e : e + SB] = jnp.where(low, t, 0.0).astype(BF16)
-                k.q[g, b, o : o + SB] = jnp.where(low, turned, 0.0).astype(BF16)
-                k.q[g, b, R * SB + e : R * SB + e + SB] = jnp.where(low, 0.0, turned).astype(BF16)
-                k.q[g, b, R * SB + o : R * SB + o + SB] = jnp.where(low, 0.0, t).astype(BF16)
+                x = jnp.transpose(k.acc[r0, at : at + LANES].astype(BF16).astype(F32) * (HD ** -0.5))
+                turned = pltpu.roll(x, SB, 1)
+                for h, (left, right) in enumerate(((x, turned), (turned, x))):
+                    y = jnp.where(tall_low, left[:HD], right[HD:]).astype(BF16)
+                    lo = slice(pair * LANES, (pair + 1) * LANES)
+                    hi = slice(R * SB + pair * LANES, R * SB + (pair + 1) * LANES)
+                    k.q_near[2 * t + h, g * HD : (g + 1) * HD, g * R * SB + pair * LANES : g * R * SB + (pair + 1) * LANES] = y
+                    k.q_far[g, 2 * t + h, :HD, lo] = y
+                    k.q_far[g, 2 * t + h, HD:, hi] = y
         return carry
 
-    lax.fori_loop(0, nb, query_step, 0)
+    lax.fori_loop(0, nb // 2, query_step, 0)
     bias_copy.wait()
     for i in range(1, n):
         req_copy(i).wait_send()
@@ -370,14 +377,6 @@
 
     k.sum_keys[...] = k.sum_key[...].astype(BF16)
     k.sum_vals[...] = jnp.transpose(k.sum_val[...]).astype(BF16)
-    span = lax.broadcasted_iota(jnp.int32, k.until.shape, 0)
-    row = lax.broadcasted_iota(jnp.int32, k.until.shape, 1) % SB
-    source, t = span // slot, span % slot
-    k.until[...] = jnp.where(
-        (t < spans) & (source <= me) & (source < n),
-        (t - spans * source) * CMP + (CMP - 1) - row, 1 << 30,
-    )
-
     def blocks_done():
         for i in range(1, n):
 
@@ -411,30 +410,42 @@
     return tiles
 
 
-def near(n, G, R, nb, k, blocks, b, carry):
+def near_scores(n, k, b):
+    own = (b + 1) * SB
+    count = n * k.sum_send.shape[0] // 2
+    keys = jnp.concatenate([k.keys[:own], k.sum_keys[:count]], axis=0)
+    k.score[b % 2, : own + count] = jnp.dot(keys, k.q_near[b], preferred_element_type=F32)
+
+
+def near(n, G, R, nb, k, b):
+    me = lax.axis_index("kv")
     width = R * SB
-    q = jnp.concatenate([k.q[g, b, g * width : (g + 1) * width] for g in range(G)], axis=0)
-    keys = blocks * SB
-    k.score[:keys] = lax.dot_general(k.keys[:keys], q, NT, preferred_element_type=F32)
-    own = pl.ds(b * SB, SB)
+    score = k.score.at[b % 2]
+    rows = slice(b * SB, (b + 1) * SB)
     shape = (SB, G * width)
     later = lax.broadcasted_iota(jnp.int32, shape, 0) > lax.broadcasted_iota(jnp.int32, shape, 1) % SB
-    k.score[own, :] += jnp.where(later, LOW, 0.0)
 
     def bias(j):
         return jnp.concatenate([jnp.full((8, width), k.bias_smem[g, b, j], F32) for g in range(G)], axis=1)
 
+    def block(j):
+        s = score[j * SB : (j + 1) * SB]
+        return s + jnp.where(later, LOW, 0.0) if j == b else s
+
     top = None
-    for j in range(blocks):
-        t = row8(k.score[j * SB : (j + 1) * SB]) + bias(j)
+    for j in range(b + 1):
+        t = row8(block(j)) + bias(j)
         top = t if top is None else jnp.maximum(top, t)
     top = jnp.max(top, axis=0, keepdims=True)
     total = jnp.zeros((8, G * width), F32)
     weights = []
-    for j in range(blocks):
-        p = jnp.exp(k.score[j * SB : (j + 1) * SB] - (top - bias(j)[:1]))
+    for j in range(b + 1):
+        p = jnp.exp(block(j) - (top - bias(j)[:1]))
         total = total + sum8(p)
         weights.append(p.astype(BF16))
+    if b % 2 == 0:
+        weights.append(jnp.zeros(shape, BF16))
+    keys = len(weights) * SB
     weights = jnp.concatenate(weights, axis=0)
     k.top[b] = jnp.broadcast_to(top, k.top.shape[1:])
     k.total[b] = total
@@ -444,23 +455,50 @@
             k.vals[g * HD : (g + 1) * HD, :keys], weights[:, cols], preferred_element_type=F32
         )
 
-    s = lax.dot_general(k.sum_keys[...], q, NT, preferred_element_type=F32)
-    until = jnp.concatenate([k.until[...]] * (G * width // LANES), axis=1)
-    s = jnp.where(until <= b * SB, s, LOW)
-    top = jnp.max(row8(s), axis=0, keepdims=True)
-    p = jnp.exp(s - top)
-    total = jnp.sum(sum8(p), axis=0, keepdims=True)
+    slot = k.sum_send.shape[0] // 2
+    spans = nb * SB // CMP
+    base = (b + 1) * SB
+    seen_shape = (slot, G * width)
+    span = lax.broadcasted_iota(jnp.int32, seen_shape, 0)
+    seen = (span < spans) & (
+        span * CMP + (CMP - 1) <= b * SB + lax.broadcasted_iota(jnp.int32, seen_shape, 1) % SB
+    )
+
+    def summary(i):
+        s = score[base + i * slot : base + (i + 1) * slot]
+        return jnp.where(seen, s, LOW) if i == 0 else s
+
+    def gone(i):
+        return jnp.where(me >= i, 0.0, LOW).astype(F32)
+
+    top = row8(summary(0))
+    for i in range(1, n):
+        top = jnp.maximum(top, row8(summary(i)) + gone(i))
+    top = jnp.max(top, axis=0, keepdims=True)
+    total = jnp.zeros((8, G * width), F32)
+    real = spans - spans // 8 * 8
+    partial = lax.broadcasted_iota(jnp.int32, (8, G * width), 0) < real
+    weights = []
+    for i in range(n):
+        p = jnp.exp(summary(i) - (top - gone(i)))
+        total = total + sum8(p[: spans // 8 * 8])
+        if real:
+            total = total + jnp.where(partial, p[spans // 8 * 8 :], 0.0)
+        weights.append(p)
+    more = k.sum_vals.shape[1] - n * slot
+    if more:
+        weights.append(jnp.zeros((more, G * width), F32))
+    weights = jnp.concatenate(weights, axis=0).astype(BF16)
+    total = jnp.sum(total, axis=0, keepdims=True)
     scale = jnp.where(top > LOW * 0.5, 1.0 / total, 0.0)
-    p = p.astype(BF16)
     outs = []
     for g in range(G):
         cols = slice(g * width, (g + 1) * width)
-        o = jnp.dot(k.sum_vals[g * HD : (g + 1) * HD, :], p[:, cols], preferred_element_type=F32)
+        o = jnp.dot(k.sum_vals[g * HD : (g + 1) * HD, :], weights[:, cols], preferred_element_type=F32)
         outs.append(o * scale[:, cols])
     for t, tile in enumerate(turn(outs)):
         cols = slice(t * LANES, (t + 1) * LANES)
-        k.mixed[own, cols] = tile * k.gate[0, own, cols]
-    return carry
+        k.mixed[rows, cols] = tile * k.gate[0, rows, cols]
 
 
 def distant(n, G, R, nb, k, b):
@@ -470,7 +508,7 @@
     for g in range(G):
         cols = slice(g * width, (g + 1) * width)
         keys = k.far[:, g, :SB, :].reshape((n - 1) * SB, LANES)
-        k.far_score[g] = lax.dot_general(keys, k.q[g, b], NT, preferred_element_type=F32)
+        k.far_score[g] = jnp.dot(keys, k.q_far[g, b], preferred_element_type=F32)
 
         def bias(i, h):
             return k.bias_smem[g, b, nb + 2 * i + h]
@@ -514,18 +552,11 @@
     step_rows = SB // 2
     att, ow = k.att, k.ow
 
-    few = (nb // 2 + 1) // 2 * 2
-
-    def near_blocks(which):
-        @pl.when(which == 0)
-        def _():
-            lax.fori_loop(0, half_blocks, functools.partial(near, n, G, R, nb, k, few), 0)
-
-        @pl.when(which == 1)
-        def _():
-            lax.fori_loop(half_blocks, nb, functools.partial(near, n, G, R, nb, k, nb), 0)
-
-    near_blocks(1 - side)
+    near_scores(n, k, 0)
+    for b in range(nb):
+        if b + 1 < nb:
+            near_scores(n, k, b + 1)
+        near(n, G, R, nb, k, b)
     for c in ow_loads:
         c.wait()
     travel.relay_x(1)
@@ -606,8 +637,12 @@
 
     def early_step(i, carry):
         early_block(i)
-        forward(i)
-        for at, relay, j in ((0, travel.relay_x, 2), (1, travel.relay_y, 0), (2, travel.relay_x, 3), (3, travel.relay_y, 1)):
+
+        @pl.when(i > 0)
+        def _():
+            forward(i - 1)
+
+        for at, relay, j in ((1, travel.relay_x, 2), (3, travel.relay_y, 0), (4, travel.relay_x, 3)):
 
             @pl.when(i == min(at, half_blocks - 1))
             def _():
@@ -616,12 +651,18 @@
         return carry
 
     lax.fori_loop(0, half_blocks, early_step, 0)
+    forward(half_blocks - 1)
 
     own_first = side * half_blocks
-    near_blocks(side)
-
+    travel.relay_y(1)
     def own_att(b, carry):
         distant(n, G, R, nb, k, b)
+        for at, j in ((2, 2), (4, 3)):
+
+            @pl.when(b == own_first + min(at, half_blocks - 1))
+            def _():
+                travel.relay_y(j)
+
         return carry
 
     lax.fori_loop(own_first, own_first + half_blocks, own_att, 0)
@@ -632,20 +673,19 @@
         device_id={"tp": partner}, device_id_type=MESH,
     )
     p_copy.start()
-    travel.relay_y(2)
 
     def own_step(j, carry):
         w = ow[:, pl.ds(pl.multiple_of(j * cw, cw), cw)]
-        theirs = att[theirs_at, :]
-        k.dsend[j] = jnp.dot(theirs, w, preferred_element_type=F32).astype(BF16)
+        k.halves[...] = jnp.dot(
+            att[pl.ds(pl.multiple_of(own_first * SB, SB), 2 * quarter), :], w, preferred_element_type=F32
+        ).astype(BF16)
+        k.dsend[j] = k.halves[pl.ds(pl.multiple_of((1 - core) * quarter, step_rows), quarter), :]
         d_copy(j).start()
-        ours = att[ours_at, :]
-        k.mine[j] = jnp.dot(ours, w, preferred_element_type=F32).astype(BF16)
+        k.mine[j] = k.halves[pl.ds(pl.multiple_of(core * quarter, step_rows), quarter), :]
         return carry
 
     lax.fori_loop(0, chunks, own_step, 0)
 
-    travel.relay_y(3)
     travel.arrived()
     p_copy.wait_recv()
     for c in range(2):
@@ -729,7 +769,8 @@
     half = nb // 2
     inputs = ["tok_hbm", "qw_hbm", "kw_hbm", "vw_hbm", "gw_hbm", "chosen", "km", "vm", "pos", "ow_hbm"]
     scratch = {
-        "q": V((G, nb, 2 * R * SB, LANES), BF16),
+        "q_near": V((nb, G * HD, G * R * SB), BF16),
+        "q_far": V((G, nb, 2 * HD, 2 * R * SB), BF16),
         "tok": V((rows, depth), BF16),
         "qw": V((depth, heads * HD), BF16),
         "kvw": V((depth, 2 * LANES), BF16),
@@ -757,14 +798,14 @@
         "sum_val": V((all_spans, LANES), F32),
         "sum_keys": V((all_spans, LANES), BF16),
         "sum_vals": V((LANES, all_spans), BF16),
-        "until": V((all_spans, LANES), jnp.int32),
-        "score": V((rows, heads * HD), F32),
+        "score": V((2, rows + n * slot, heads * HD), F32),
         "far_score": V((G, (n - 1) * SB, 2 * R * SB), F32),
         "top": V((nb, 8, heads * HD), F32),
         "total": V((nb, 8, heads * HD), F32),
         "part": V((nb, HD, heads * HD), F32),
         "mixed": V((rows, heads * HD), F32),
         "att": V((rows, heads * HD), BF16),
+        "halves": V((2 * quarter, cw), BF16),
         "mine": V((oc, quarter, cw), BF16),
         "dsend": V((oc, quarter, cw), BF16),
         "drecv": V((oc, quarter, cw), BF16),

time: 57.5 us -> 54.7 us (0.951)
  Pallas kernels: 56.2 us -> 53.4 us
    pallas_call x1, Pallas kernels: 56.2 us -> 53.4 us  [local(): pl.pallas_call(functools.partial(layer_kernel, n, G, R, nb, kc, cw, input...]
where the time goes in v2:
time: 54.7 us; the launch traced here: 54.5 us
  Pallas kernels  53.4 us (98%)
  local copies, waits for them, and re-layouts  1.06 us (2%)
    pallas_call x1, Pallas kernels, local(): pl.pallas_call(functools.partial(layer_kernel, n, G, R, nb, kc, cw, input...  53.4 us

profile of v2, /device:TPU:1, one launch (start us, length us, event | category | flops | bytes accessed | tf_op | source)
XLA Modules:
  0.0 54.5 jit_solution(4066078788471956919)
XLA Ops:
  0.0 53.4 %layer.1 = bf16[160,4096]{1,0:T(8,128)(2,1)S(1)} custom-call(bf16[640,4096]{1,0:T(8,128)(2,1)} %refs_0_.1, bf16[4096,512]{1,0:T(8,128)(2,1)} %refs_1_.1, bf16[4096,128]{1,0:T(8,128)(2,1)} %refs_2_.1, bf16[4096,128]{1,0:T(8,128)(2,1)} %refs_3_.1, bf16[64,4096]{1,0:T(8,128)(2,1)} %bitcast.3, s32[10,2,16]{2,1,0:T(2,128)} %refs_5_.1, bf16[8,32]{1,0:T(8,128)(2,1)} %bitcast.4, ...), custom_call_target="tpu_custom_call" | custom-call | tf_op jit(solution)/shard_map/layer/pallas_call | solution.py:834
  53.4 1.1 %copy.12 = bf16[160,4096]{1,0:T(8,128)(2,1)} copy(bf16[160,4096]{1,0:T(8,128)(2,1)S(1)} %layer.1) | data formatting | bytes 2621440

commit v3 on v2

--- a/solution.py
+++ b/solution.py
@@ -13,7 +13,6 @@
 SB = 64
 N_SEL = 16
 LANES = 128
-PIECES = 4
 LOW = -1e30
 F32 = jnp.float32
 BF16 = jnp.bfloat16
@@ -66,21 +65,28 @@
 
 
 class Travel:
-    def __init__(self, k, pieces):
+    SPLIT = ((0, 2), (2, 1), (3, 2))
+
+    def __init__(self, k):
         tp, me = lax.axis_index("tp"), lax.axis_index("kv")
         core, side = lax.rem(tp, 2), tp // 2
-        self.k, self.pieces = k, pieces
+        place = lax.rem(me, 4)
+        odd, upper = lax.rem(place, 2), place // 2
+        self.k = k
         self.across = {"tp": (1 - side) * 2 + core}
         self.partner = {"tp": side * 2 + 1 - core}
-        self.beside = {"kv": me + 1 - 2 * lax.rem(me, 2)}
-        self.mine = lax.rem(me, 2)
+        self.first_of = {"kv": me + 1 - 2 * odd}
+        self.second_of = {"kv": me + 2 - 4 * upper}
+        self.own, self.by_first, self.by_second, self.last = (
+            place, place + 1 - 2 * odd, place + 2 - 4 * upper, 3 - place,
+        )
         self.columns = k.wfar.shape[2]
         self.first = k.ow.shape[1] - self.columns
-        self.size = self.columns // 2 // pieces
-
-    def cols(self, half, j, base=0):
-        at = base + half * (self.columns // 2) + j * self.size
-        return pl.ds(pl.multiple_of(at, LANES), self.size)
+
+    def cols(self, quarter, j, base=0):
+        unit = self.columns // 20
+        at, size = self.SPLIT[j]
+        return pl.ds(pl.multiple_of(base + (quarter * 5 + at) * unit, LANES), size * unit)
 
     def copy(self, src, dst, send, recv, target):
         return pltpu.make_async_remote_copy(
@@ -90,8 +96,9 @@
 
     def x(self, j):
         k = self.k
+        quarter, piece = (self.own, j) if j < 3 else (self.last, 2)
         return self.copy(
-            k.ow_hbm.at[:, self.cols(self.mine, j, self.first)], k.wfar.at[1, :, self.cols(self.mine, j)],
+            k.ow_hbm.at[:, self.cols(quarter, piece, self.first)], k.wfar.at[1, :, self.cols(quarter, piece)],
             k.wx_s.at[j], k.wx_r.at[j], self.across,
         )
 
@@ -101,48 +108,71 @@
             k.ow_hbm.at[:, pl.ds(self.first, self.columns)], k.wfar.at[0], k.wp_s, k.wp_r, self.partner
         )
 
-    def y(self, j):
-        here = self.k.wfar.at[1, :, self.cols(self.mine, j)]
-        return self.copy(here, here, self.k.wy_s.at[j], self.k.wy_r.at[j], self.beside)
-
-    def y_arrival(self, j):
-        here = self.k.wfar.at[1, :, self.cols(1 - self.mine, j)]
-        return self.copy(here, here, self.k.wy_s.at[j], self.k.wy_r.at[j], self.beside)
-
-    def d(self, h, j):
+    def pass_on(self, quarter, j, sems, at, target):
+        here = self.k.wfar.at[1, :, self.cols(quarter, j)]
+        return self.copy(here, here, sems[0].at[at], sems[1].at[at], target)
+
+    def y(self, j, arrival=False):
+        return self.pass_on(self.by_first if arrival else self.own, j, (self.k.wy_s, self.k.wy_r), j, self.first_of)
+
+    def z(self, j, arrival=False):
+        return self.pass_on(self.by_second if arrival else self.own, j, (self.k.wz_s, self.k.wz_r), j, self.second_of)
+
+    def g(self, j, arrival=False):
+        return self.pass_on(self.last if arrival else self.by_second, j, (self.k.wg_s, self.k.wg_r), j, self.first_of)
+
+    def d(self, q, j):
         k = self.k
-        at = self.cols(self.mine if h == 0 else 1 - self.mine, j)
+        at = self.cols((self.own, self.by_first, self.by_second, self.last)[q], j)
         return self.copy(
-            k.wfar.at[1, :, at], k.wfar.at[2, :, at], k.wd_s.at[h, j], k.wd_r.at[h, j], self.partner
+            k.wfar.at[1, :, at], k.wfar.at[2, :, at], k.wd_s.at[q, j], k.wd_r.at[q, j], self.partner
         )
 
     def start(self):
-        for j in range(self.pieces):
+        for j in range(4):
             self.x(j).start()
         self.p().start()
 
     def relay_x(self, j):
         self.x(j).wait_recv()
-        self.y(j).start()
-        self.d(0, j).start()
+        if j < 3:
+            self.z(j).start()
+            self.y(j).start()
+            self.d(0, j).start()
+        else:
+            self.d(3, 2).start()
 
     def relay_y(self, j):
-        self.y_arrival(j).wait_recv()
+        self.y(j, True).wait_recv()
         self.d(1, j).start()
+
+    def relay_z(self, j):
+        self.z(j, True).wait_recv()
+        if j < 2:
+            self.g(j).start()
+        self.d(2, j).start()
+
+    def relay_g(self, j):
+        self.g(j, True).wait_recv()
+        self.d(3, j).start()
 
     def arrived(self):
         self.p().wait_recv()
-        for h in range(2):
-            for j in range(self.pieces):
-                self.d(h, j).wait_recv()
+        for q in range(4):
+            for j in range(3):
+                self.d(q, j).wait_recv()
 
     def sent(self):
         self.p().wait_send()
-        for j in range(self.pieces):
+        for j in range(4):
             self.x(j).wait_send()
+        for j in range(3):
             self.y(j).wait_send()
-            for h in range(2):
-                self.d(h, j).wait_send()
+            self.z(j).wait_send()
+            if j < 2:
+                self.g(j).wait_send()
+            for q in range(4):
+                self.d(q, j).wait_send()
 
 
 def project(n, G, R, nb, kc, k, ow_loads, travel):
@@ -173,6 +203,14 @@
             pltpu.make_async_copy(k.gw_hbm.at[:, part(i)], k.gw.at[pl.ds(half_gates, half_gates), part(i)], k.sem_gw.at[1, i]),
         ]
 
+    small = [
+        pltpu.make_async_copy(src, dst, k.sem_small.at[i])
+        for i, (src, dst) in enumerate((
+            (k.chosen_hbm, k.chosen), (k.km_hbm, k.km), (k.vm_hbm, k.vm), (k.pos_hbm, k.pos),
+        ))
+    ]
+    for c in small:
+        c.start()
     for i in range(chunks):
         for c in loads(i):
             c.start()
@@ -185,6 +223,7 @@
     for i in range(1, 4):
         pl.semaphore_signal(barrier, inc=1, device_id={"tp": lax.rem(tp + i, 4)}, device_id_type=MESH)
 
+    small[0].wait()
     requests(n, G, nb, k)
     pl.semaphore_wait(barrier, n + 2)
 
@@ -242,6 +281,8 @@
     lax.fori_loop(0, chunks, kv_step, 0)
     for c in ow_loads:
         c.start()
+    for c in small[1:]:
+        c.wait()
     low = lax.broadcasted_iota(jnp.int32, (SB, LANES), 1) < HD
     mix_row = lax.broadcasted_iota(jnp.int32, k.km.shape, 0)
     mix_low = lax.broadcasted_iota(jnp.int32, (CMP, LANES), 1) < HD
@@ -360,6 +401,7 @@
         return carry
 
     lax.fori_loop(0, nb // 2, query_step, 0)
+    travel.relay_x(1)
     bias_copy.wait()
     for i in range(1, n):
         req_copy(i).wait_send()
@@ -559,7 +601,7 @@
         near(n, G, R, nb, k, b)
     for c in ow_loads:
         c.wait()
-    travel.relay_x(1)
+    travel.relay_x(2)
     blocks_done()
 
     def d_copy(j):
@@ -616,17 +658,11 @@
         for h in range(2):
             a_copy(2 * i + h).start()
         a = att[pl.ds((other_first + i) * SB, SB), :]
-        for j in range(side_cols // cw):
-            cols = pl.ds(pl.multiple_of((1 - core) * side_cols + j * cw, cw), cw)
-            k.esend[i, :, j * cw : (j + 1) * cw] = jnp.dot(
-                a, ow[:, cols], preferred_element_type=F32
-            ).astype(BF16)
+        cols = pl.ds(pl.multiple_of((1 - core) * side_cols, LANES), side_cols)
+        k.esend[i] = jnp.dot(a, ow[:, cols], preferred_element_type=F32).astype(BF16)
         e_copy(i).start()
-        for j in range(side_cols // cw):
-            cols = pl.ds(pl.multiple_of(core * side_cols + j * cw, cw), cw)
-            k.early[i, :, j * cw : (j + 1) * cw] = jnp.dot(
-                a, ow[:, cols], preferred_element_type=F32
-            ).astype(BF16)
+        cols = pl.ds(pl.multiple_of(core * side_cols, LANES), side_cols)
+        k.early[i] = jnp.dot(a, ow[:, cols], preferred_element_type=F32).astype(BF16)
 
     def forward(i):
         e_copy(i).wait_recv()
@@ -642,11 +678,17 @@
         def _():
             forward(i - 1)
 
-        for at, relay, j in ((1, travel.relay_x, 2), (3, travel.relay_y, 0), (4, travel.relay_x, 3)):
+        for at, relays in (
+            (1, ((travel.relay_x, 3), (travel.relay_y, 0))),
+            (2, ((travel.relay_y, 1),)),
+            (3, ((travel.relay_z, 0),)),
+            (4, ((travel.relay_z, 1), (travel.relay_y, 2))),
+        ):
 
             @pl.when(i == min(at, half_blocks - 1))
             def _():
-                relay(j)
+                for relay, j in relays:
+                    relay(j)
 
         return carry
 
@@ -654,14 +696,17 @@
     forward(half_blocks - 1)
 
     own_first = side * half_blocks
-    travel.relay_y(1)
     def own_att(b, carry):
         distant(n, G, R, nb, k, b)
-        for at, j in ((2, 2), (4, 3)):
+        for at, relays in (
+            (3, ((travel.relay_g, 0), (travel.relay_z, 2))),
+            (4, ((travel.relay_g, 1),)),
+        ):
 
             @pl.when(b == own_first + min(at, half_blocks - 1))
             def _():
-                travel.relay_y(j)
+                for relay, j in relays:
+                    relay(j)
 
         return carry
 
@@ -732,7 +777,7 @@
 def layer_kernel(n, G, R, nb, kc, cw, names, *refs):
     k = types.SimpleNamespace(**dict(zip(names, refs, strict=True)))
     ow_loads = [pltpu.make_async_copy(k.ow_hbm, k.ow, k.sem_ow)]
-    travel = Travel(k, PIECES)
+    travel = Travel(k)
     blocks_done = project(n, G, R, nb, kc, k, ow_loads, travel)
     attend_and_mix(n, G, R, nb, cw, k, ow_loads, blocks_done, travel)
 
@@ -754,11 +799,11 @@
     chunks = depth // kc
     width = out_weight.shape[1]
     cw = 512
-    wide = width // 2
+    wide = width // (20 * LANES * 8 // 5) * 20 * LANES
     summed = width - wide
     oc = summed // cw
     gates_all = gate_weight.shape[1]
-    assert G == 2 and n % 2 == 0 and 2 * gates_all == LANES and nb % 2 == 0
+    assert G == 2 and n % 4 == 0 and 2 * gates_all == LANES and nb % 2 == 0
 
     vmem = pl.BlockSpec(memory_space=pltpu.VMEM)
     hbm = pl.BlockSpec(memory_space=pl.ANY)
@@ -767,10 +812,15 @@
     nbp = -(-nb // 8) * 8
     quarter = rows // 4
     half = nb // 2
-    inputs = ["tok_hbm", "qw_hbm", "kw_hbm", "vw_hbm", "gw_hbm", "chosen", "km", "vm", "pos", "ow_hbm"]
+    inputs = ["tok_hbm", "qw_hbm", "kw_hbm", "vw_hbm", "gw_hbm", "chosen_hbm", "km_hbm", "vm_hbm", "pos_hbm", "ow_hbm"]
     scratch = {
         "q_near": V((nb, G * HD, G * R * SB), BF16),
         "q_far": V((G, nb, 2 * HD, 2 * R * SB), BF16),
+        "chosen": V(chosen.shape, jnp.int32),
+        "km": V(key_mixing.shape[::-1], BF16),
+        "vm": V(value_mixing.shape[::-1], BF16),
+        "pos": V(summary_pos.shape, BF16),
+        "sem_small": dma((4,)),
         "tok": V((rows, depth), BF16),
         "qw": V((depth, heads * HD), BF16),
         "kvw": V((depth, 2 * LANES), BF16),
@@ -827,15 +877,15 @@
         "d_s": dma((oc,)), "d_r": dma((oc,)), "e_s": dma((half,)), "e_r": dma((half,)),
         "x_s": dma((2 * half,)), "x_r": dma((2, half)),
         "a_s": dma((2 * half,)), "a_r": dma((2, half)), "p_s": dma, "p_r": dma,
-        "wx_s": dma((PIECES,)), "wx_r": dma((PIECES,)), "wp_s": dma, "wp_r": dma,
-        "wy_s": dma((PIECES,)), "wy_r": dma((PIECES,)),
-        "wd_s": dma((2, PIECES)), "wd_r": dma((2, PIECES)),
+        "wx_s": dma((4,)), "wx_r": dma((4,)), "wp_s": dma, "wp_r": dma,
+        "wy_s": dma((3,)), "wy_r": dma((3,)), "wz_s": dma((3,)), "wz_r": dma((3,)),
+        "wg_s": dma((2,)), "wg_r": dma((2,)), "wd_s": dma((4, 3)), "wd_r": dma((4, 3)),
     }
     return pl.pallas_call(
         functools.partial(layer_kernel, n, G, R, nb, kc, cw, inputs + ["out"] + list(scratch)),
         name="layer",
         out_shape=pltpu.VMEM((quarter, width), BF16),
-        in_specs=[hbm] * 5 + [vmem] * 4 + [hbm],
+        in_specs=[hbm] * 10,
         out_specs=vmem,
         scratch_shapes=list(scratch.values()),
         compiler_params=pltpu.CompilerParams(

time: 54.7 us -> 48.7 us (0.89)
  Pallas kernels: 53.4 us -> 47.3 us
    pallas_call x1, Pallas kernels: 53.4 us -> 47.3 us  [local(): pl.pallas_call(functools.partial(layer_kernel, n, G, R, nb, kc, cw, input...]
where the time goes in v3:
time: 48.7 us; the launch traced here: 48.4 us
  Pallas kernels  47.3 us (97%)
  local copies, waits for them, and re-layouts  1.06 us (2%)
    pallas_call x1, Pallas kernels, local(): pl.pallas_call(functools.partial(layer_kernel, n, G, R, nb, kc, cw, input...  47.3 us
    unnamed x1, local copies, waits for them, and re-layouts  1.06 us

profile of v3, /device:TPU:1, one launch (start us, length us, event | category | flops | bytes accessed | tf_op | source)
XLA Modules:
  0.0 48.4 jit_solution(17606513594521400260)
XLA Ops:
  0.0 47.3 %layer.1 = bf16[160,4096]{1,0:T(8,128)(2,1)S(1)} custom-call(bf16[640,4096]{1,0:T(8,128)(2,1)} %refs_0_.1, bf16[4096,512]{1,0:T(8,128)(2,1)} %refs_1_.1, bf16[4096,128]{1,0:T(8,128)(2,1)} %refs_2_.1, bf16[4096,128]{1,0:T(8,128)(2,1)} %refs_3_.1, bf16[64,4096]{1,0:T(8,128)(2,1)} %bitcast.3, s32[10,2,16]{2,1,0:T(2,128)} %refs_5_.1, bf16[8,32]{1,0:T(8,128)(2,1)} %bitcast.4, ...), custom_call_target="tpu_custom_call" | custom-call | tf_op jit(solution)/shard_map/layer/pallas_call | solution.py:884
  47.3 1.1 %copy.12 = bf16[160,4096]{1,0:T(8,128)(2,1)} copy(bf16[160,4096]{1,0:T(8,128)(2,1)S(1)} %layer.1) | data formatting | bytes 2621440

commit v4 on v3

--- a/solution.py
+++ b/solution.py
@@ -19,6 +19,10 @@
 MESH = pl.DeviceIdType.MESH
 VMEM_LIMIT = 64_000_000
 NT = (((1,), (1,)), ((), ()))
+
+
+def all_sent(ref, sem):
+    pltpu.make_async_copy(ref, ref, sem).wait()
 
 
 def requests(n, G, nb, k):
@@ -99,7 +103,7 @@
         quarter, piece = (self.own, j) if j < 3 else (self.last, 2)
         return self.copy(
             k.ow_hbm.at[:, self.cols(quarter, piece, self.first)], k.wfar.at[1, :, self.cols(quarter, piece)],
-            k.wx_s.at[j], k.wx_r.at[j], self.across,
+            k.wx_s, k.wx_r.at[j], self.across,
         )
 
     def p(self):
@@ -110,7 +114,7 @@
 
     def pass_on(self, quarter, j, sems, at, target):
         here = self.k.wfar.at[1, :, self.cols(quarter, j)]
-        return self.copy(here, here, sems[0].at[at], sems[1].at[at], target)
+        return self.copy(here, here, sems[0], sems[1].at[at], target)
 
     def y(self, j, arrival=False):
         return self.pass_on(self.by_first if arrival else self.own, j, (self.k.wy_s, self.k.wy_r), j, self.first_of)
@@ -125,7 +129,7 @@
         k = self.k
         at = self.cols((self.own, self.by_first, self.by_second, self.last)[q], j)
         return self.copy(
-            k.wfar.at[1, :, at], k.wfar.at[2, :, at], k.wd_s.at[q, j], k.wd_r.at[q, j], self.partner
+            k.wfar.at[1, :, at], k.wfar.at[2, :, at], k.wd_s, k.wd_r.at[q], self.partner
         )
 
     def start(self):
@@ -156,23 +160,19 @@
         self.g(j, True).wait_recv()
         self.d(3, j).start()
 
-    def arrived(self):
-        self.p().wait_recv()
-        for q in range(4):
-            for j in range(3):
-                self.d(q, j).wait_recv()
+    def quarter(self, q, base=0):
+        unit = self.columns // 20
+        at = base + (self.own, self.by_first, self.by_second, self.last)[q] * 5 * unit
+        return pl.ds(pl.multiple_of(at, LANES), 5 * unit)
+
+    def arrived(self, q):
+        all_sent(self.k.wfar.at[2, :, self.quarter(q)], self.k.wd_r.at[q])
 
     def sent(self):
+        k, unit = self.k, self.columns // 20
         self.p().wait_send()
-        for j in range(4):
-            self.x(j).wait_send()
-        for j in range(3):
-            self.y(j).wait_send()
-            self.z(j).wait_send()
-            if j < 2:
-                self.g(j).wait_send()
-            for q in range(4):
-                self.d(q, j).wait_send()
+        for sem, size in ((k.wx_s, 7), (k.wy_s, 5), (k.wz_s, 5), (k.wg_s, 3), (k.wd_s, 20)):
+            all_sent(k.wfar.at[1, :, pl.ds(0, size * unit)], sem)
 
 
 def project(n, G, R, nb, kc, k, ow_loads, travel):
@@ -198,9 +198,9 @@
 
     def late(i):
         return [
-            pltpu.make_async_copy(k.qw_hbm.at[part(i)], k.qw.at[part(i)], k.sem_qw.at[i]),
-            pltpu.make_async_copy(k.gw_hbm.at[:, part(i)], k.gw.at[pl.ds(0, half_gates), part(i)], k.sem_gw.at[0, i]),
-            pltpu.make_async_copy(k.gw_hbm.at[:, part(i)], k.gw.at[pl.ds(half_gates, half_gates), part(i)], k.sem_gw.at[1, i]),
+            pltpu.make_async_copy(k.qw_hbm.at[part(i)], k.qw.at[part(i)], k.sem_tok.at[i]),
+            pltpu.make_async_copy(k.gw_hbm.at[:, part(i)], k.gw.at[pl.ds(0, half_gates), part(i)], k.sem_kw.at[i]),
+            pltpu.make_async_copy(k.gw_hbm.at[:, part(i)], k.gw.at[pl.ds(half_gates, half_gates), part(i)], k.sem_vw.at[i]),
         ]
 
     small = [
@@ -230,7 +230,7 @@
     def req_copy(i):
         return pltpu.make_async_remote_copy(
             src_ref=k.req.at[lax.rem(me + n - i, n)], dst_ref=k.req_in.at[i],
-            send_sem=k.req_s.at[i], recv_sem=k.req_r.at[i],
+            send_sem=k.req_s, recv_sem=k.req_r.at[i],
             device_id={"kv": lax.rem(me + n - i, n)}, device_id_type=MESH,
         )
 
@@ -403,8 +403,8 @@
     lax.fori_loop(0, nb // 2, query_step, 0)
     travel.relay_x(1)
     bias_copy.wait()
+    all_sent(k.req.at[pl.ds(0, n - 1)], k.req_s)
     for i in range(1, n):
-        req_copy(i).wait_send()
 
         @pl.when(me + i < n)
         def _():
@@ -543,14 +543,18 @@
         k.mixed[rows, cols] = tile * k.gate[0, rows, cols]
 
 
-def distant(n, G, R, nb, k, b):
+def far_scores(n, G, k, b, at):
+    for g in range(G):
+        keys = k.far[:, g, :SB, :].reshape((n - 1) * SB, LANES)
+        k.far_score[at, g] = jnp.dot(keys, k.q_far[g, b], preferred_element_type=F32)
+
+
+def distant(n, G, R, nb, k, b, at):
     width = R * SB
-    own = pl.ds(b * SB, SB)
+    own = pl.ds(pl.multiple_of(b * SB, SB), SB)
     outs = []
     for g in range(G):
         cols = slice(g * width, (g + 1) * width)
-        keys = k.far[:, g, :SB, :].reshape((n - 1) * SB, LANES)
-        k.far_score[g] = jnp.dot(keys, k.q_far[g, b], preferred_element_type=F32)
 
         def bias(i, h):
             return k.bias_smem[g, b, nb + 2 * i + h]
@@ -558,7 +562,7 @@
         before = k.top[b, :1, cols]
         top = jnp.broadcast_to(before, (8, width))
         for i in range(n - 1):
-            t = row8(k.far_score[g, i * SB : (i + 1) * SB])
+            t = row8(k.far_score[at, g, i * SB : (i + 1) * SB])
             for h in range(2):
                 top = jnp.maximum(top, t[:, h * width : (h + 1) * width] + bias(i, h))
         top = jnp.max(top, axis=0, keepdims=True)
@@ -567,7 +571,7 @@
         weights = []
         for i in range(n - 1):
             for h in range(2):
-                s = k.far_score[g, i * SB : (i + 1) * SB, h * width : (h + 1) * width]
+                s = k.far_score[at, g, i * SB : (i + 1) * SB, h * width : (h + 1) * width]
                 p = jnp.exp(s - (top - bias(i, h)))
                 total = total + sum8(p)
                 weights.append(p.astype(BF16))
@@ -607,54 +611,51 @@
     def d_copy(j):
         return pltpu.make_async_remote_copy(
             src_ref=k.dsend.at[j], dst_ref=k.drecv.at[j],
-            send_sem=k.d_s.at[j], recv_sem=k.d_r.at[j],
+            send_sem=k.d_s, recv_sem=k.d_r,
             device_id={"tp": partner}, device_id_type=MESH,
         )
 
     def e_copy(i):
         return pltpu.make_async_remote_copy(
             src_ref=k.esend.at[i], dst_ref=k.erecv.at[i],
-            send_sem=k.e_s.at[i], recv_sem=k.e_r.at[i],
+            send_sem=k.e_s, recv_sem=k.e_r.at[i],
             device_id={"tp": partner}, device_id_type=MESH,
         )
 
     def x_copy(i):
-        step = lax.rem(i, half_blocks)
+        step = i % half_blocks
         return pltpu.make_async_remote_copy(
             src_ref=k.xsend.at[i], dst_ref=k.xrecv.at[core, step],
-            send_sem=k.x_s.at[i], recv_sem=k.x_r.at[core, step],
+            send_sem=k.x_s, recv_sem=k.x_r,
             device_id={"tp": (1 - side) * 2 + i // half_blocks}, device_id_type=MESH,
         )
 
-    def x_arrival(c, step):
-        return pltpu.make_async_remote_copy(
-            src_ref=k.xsend.at[step], dst_ref=k.xrecv.at[c, step],
-            send_sem=k.x_s.at[step], recv_sem=k.x_r.at[c, step],
-            device_id={"tp": (1 - side) * 2 + core}, device_id_type=MESH,
-        )
-
     other_first = (1 - side) * half_blocks
 
     def a_copy(i):
-        to, step = i // half_blocks, lax.rem(i, half_blocks)
+        to, step = i // half_blocks, i % half_blocks
         rows_of = pl.ds(pl.multiple_of(other_first * SB + i * step_rows, step_rows), step_rows)
         into = pl.ds(pl.multiple_of(step * step_rows, step_rows), step_rows)
         return pltpu.make_async_remote_copy(
             src_ref=att.at[rows_of], dst_ref=k.att_in.at[1 + lax.rem(to + core, 2), into],
-            send_sem=k.a_s.at[i], recv_sem=k.a_r.at[core, step],
+            send_sem=k.a_s, recv_sem=k.a_r,
             device_id={"tp": (1 - side) * 2 + to}, device_id_type=MESH,
         )
 
-    def a_arrival(c, step):
-        into = pl.ds(pl.multiple_of(step * step_rows, step_rows), step_rows)
-        return pltpu.make_async_remote_copy(
-            src_ref=att.at[into], dst_ref=k.att_in.at[1 + lax.rem(c + core, 2), into],
-            send_sem=k.a_s.at[step], recv_sem=k.a_r.at[c, step],
-            device_id={"tp": (1 - side) * 2 + core}, device_id_type=MESH,
-        )
+    own_first = side * half_blocks
+
+    def block(i):
+        first = other_first if i < half_blocks else own_first
+        return first + i % half_blocks
+
+    def attend(i):
+        ahead = k.far_score.shape[0] - 1
+        if i + ahead < nb and (ahead or i):
+            far_scores(n, G, k, block(i + ahead), (i + ahead) % (ahead + 1))
+        distant(n, G, R, nb, k, block(i), i % (ahead + 1))
 
     def early_block(i):
-        distant(n, G, R, nb, k, other_first + i)
+        attend(i)
         for h in range(2):
             a_copy(2 * i + h).start()
         a = att[pl.ds((other_first + i) * SB, SB), :]
@@ -671,46 +672,29 @@
             k.xsend[2 * i + h] = (k.early[i, r].astype(F32) + k.erecv[i, r].astype(F32)).astype(BF16)
             x_copy(2 * i + h).start()
 
-    def early_step(i, carry):
-        early_block(i)
-
-        @pl.when(i > 0)
-        def _():
-            forward(i - 1)
-
-        for at, relays in (
-            (1, ((travel.relay_x, 3), (travel.relay_y, 0))),
-            (2, ((travel.relay_y, 1),)),
-            (3, ((travel.relay_z, 0),)),
-            (4, ((travel.relay_z, 1), (travel.relay_y, 2))),
-        ):
-
-            @pl.when(i == min(at, half_blocks - 1))
-            def _():
-                for relay, j in relays:
-                    relay(j)
-
-        return carry
-
-    lax.fori_loop(0, half_blocks, early_step, 0)
-    forward(half_blocks - 1)
-
-    own_first = side * half_blocks
-    def own_att(b, carry):
-        distant(n, G, R, nb, k, b)
-        for at, relays in (
-            (3, ((travel.relay_g, 0), (travel.relay_z, 2))),
-            (4, ((travel.relay_g, 1),)),
-        ):
-
-            @pl.when(b == own_first + min(at, half_blocks - 1))
-            def _():
-                for relay, j in relays:
-                    relay(j)
-
-        return carry
-
-    lax.fori_loop(own_first, own_first + half_blocks, own_att, 0)
+    relays = {
+        1: ((travel.relay_x, 3), (travel.relay_y, 0)),
+        2: ((travel.relay_y, 1),),
+        3: ((travel.relay_z, 0),),
+        4: ((travel.relay_z, 1), (travel.relay_y, 2)),
+        8: ((travel.relay_g, 0), (travel.relay_z, 2)),
+        9: ((travel.relay_g, 1),),
+    }
+    far_scores(n, G, k, block(0), 0)
+    for i in range(nb):
+        if i < half_blocks:
+            early_block(i)
+            if i > 0:
+                forward(i - 1)
+        else:
+            attend(i)
+        if i == half_blocks - 1:
+            forward(i)
+        for relay, j in relays.pop(i, ()):
+            relay(j)
+    for late in relays.values():
+        for relay, j in late:
+            relay(j)
     theirs_at = pl.ds(pl.multiple_of(own_first * SB + (1 - core) * quarter, step_rows), quarter)
     ours_at = pl.ds(pl.multiple_of(own_first * SB + core * quarter, step_rows), quarter)
     p_copy = pltpu.make_async_remote_copy(
@@ -731,45 +715,40 @@
 
     lax.fori_loop(0, chunks, own_step, 0)
 
-    travel.arrived()
     p_copy.wait_recv()
-    for c in range(2):
-        for step in range(half_blocks):
-            a_arrival(c, step).wait_recv()
-
-    def wide_step(j, carry):
-        cols = pl.ds(pl.multiple_of(j * cw, cw), cw)
-        out_cols = pl.ds(pl.multiple_of(travel.first + j * cw, cw), cw)
+    all_sent(k.att_in.at[pl.ds(1, 2)], k.a_r)
+    for q in range(4):
+        travel.arrived(q)
+        if q == 0:
+            travel.p().wait_recv()
+        cols, out_cols = travel.quarter(q), travel.quarter(q, travel.first)
         o = jnp.dot(att[ours_at, :], ow[:, out_cols], preferred_element_type=F32)
         for slot in range(3):
             o = o + jnp.dot(k.att_in[slot], k.wfar[slot, :, cols], preferred_element_type=F32)
         k.out[:, out_cols] = o.astype(BF16)
-        return carry
-
-    lax.fori_loop(0, travel.columns // cw, wide_step, 0)
+    all_sent(k.drecv, k.d_r)
+    all_sent(k.dsend, k.d_s)
+
     def base_step(j, carry):
-        d_copy(j).wait_recv()
         cols = pl.ds(pl.multiple_of(j * cw, cw), cw)
         k.base[:, cols] = k.mine[j].astype(F32) + k.drecv[j].astype(F32)
-        d_copy(j).wait_send()
         return carry
 
     lax.fori_loop(0, chunks, base_step, 0)
+
+    all_sent(k.xrecv, k.x_r)
 
     def last_step(s, carry):
         r = pl.ds(pl.multiple_of(s * step_rows, step_rows), step_rows)
         for c in range(2):
-            x_arrival(c, s).wait_recv()
             cols = slice(c * side_cols, (c + 1) * side_cols)
             k.out[r, cols] = (k.base[r, cols] + k.xrecv[c, s].astype(F32)).astype(BF16)
-        e_copy(s).wait_send()
-        x_copy(s).wait_send()
-        x_copy(half_blocks + s).wait_send()
-        a_copy(s).wait_send()
-        a_copy(half_blocks + s).wait_send()
         return carry
 
     lax.fori_loop(0, half_blocks, last_step, 0)
+    all_sent(k.esend, k.e_s)
+    all_sent(k.xsend, k.x_s)
+    all_sent(att.at[pl.ds(0, 2 * quarter)], k.a_s)
     p_copy.wait_send()
     travel.sent()
 
@@ -849,7 +828,7 @@
         "sum_keys": V((all_spans, LANES), BF16),
         "sum_vals": V((LANES, all_spans), BF16),
         "score": V((2, rows + n * slot, heads * HD), F32),
-        "far_score": V((G, (n - 1) * SB, 2 * R * SB), F32),
+        "far_score": V((2 if n <= 16 else 1, G, (n - 1) * SB, 2 * R * SB), F32),
         "top": V((nb, 8, heads * HD), F32),
         "total": V((nb, 8, heads * HD), F32),
         "part": V((nb, HD, heads * HD), F32),
@@ -871,15 +850,13 @@
         "sem_bias": dma,
         "sem_req": dma((n,)),
         "sem_tok": dma((chunks,)), "sem_kw": dma((chunks,)), "sem_vw": dma((chunks,)),
-        "sem_qw": dma((chunks,)), "sem_gw": dma((2, chunks)),
-        "req_s": dma((n,)), "req_r": dma((n,)), "blk_s": dma((n,)), "blk_r": dma((n,)),
+        "req_s": dma, "req_r": dma((n,)), "blk_s": dma((n,)), "blk_r": dma((n,)),
         "sum_s": dma((n,)), "sum_r": dma((n,)),
-        "d_s": dma((oc,)), "d_r": dma((oc,)), "e_s": dma((half,)), "e_r": dma((half,)),
-        "x_s": dma((2 * half,)), "x_r": dma((2, half)),
-        "a_s": dma((2 * half,)), "a_r": dma((2, half)), "p_s": dma, "p_r": dma,
-        "wx_s": dma((4,)), "wx_r": dma((4,)), "wp_s": dma, "wp_r": dma,
-        "wy_s": dma((3,)), "wy_r": dma((3,)), "wz_s": dma((3,)), "wz_r": dma((3,)),
-        "wg_s": dma((2,)), "wg_r": dma((2,)), "wd_s": dma((4, 3)), "wd_r": dma((4, 3)),
+        "d_s": dma, "d_r": dma, "e_s": dma, "e_r": dma((half,)), "x_s": dma, "x_r": dma,
+        "a_s": dma, "a_r": dma, "p_s": dma, "p_r": dma,
+        "wx_s": dma, "wx_r": dma((4,)), "wp_s": dma, "wp_r": dma,
+        "wy_s": dma, "wy_r": dma((3,)), "wz_s": dma, "wz_r": dma((3,)),
+        "wg_s": dma, "wg_r": dma((2,)), "wd_s": dma, "wd_r": dma((4,)),
     }
     return pl.pallas_call(
         functools.partial(layer_kernel, n, G, R, nb, kc, cw, inputs + ["out"] + list(scratch)),

time: 48.7 us -> 47.6 us (0.977)
  Pallas kernels: 47.3 us -> 46.2 us
    pallas_call x1, Pallas kernels: 47.3 us -> 46.2 us  [local(): pl.pallas_call(functools.partial(layer_kernel, n, G, R, nb, kc, cw, input...]
where the time goes in v4:
time: 47.6 us; the launch traced here: 47.3 us
  Pallas kernels  46.2 us (97%)
  local copies, waits for them, and re-layouts  1.06 us (2%)
    pallas_call x1, Pallas kernels, local(): pl.pallas_call(functools.partial(layer_kernel, n, G, R, nb, kc, cw, input...  46.2 us
    unnamed x1, local copies, waits for them, and re-layouts  1.06 us

profile of v4, /device:TPU:1, one launch (start us, length us, event | category | flops | bytes accessed | tf_op | source)
XLA Modules:
  0.0 47.3 jit_solution(10998560325210435635)
XLA Ops:
  0.0 46.2 %layer.1 = bf16[160,4096]{1,0:T(8,128)(2,1)S(1)} custom-call(bf16[640,4096]{1,0:T(8,128)(2,1)} %refs_0_.1, bf16[4096,512]{1,0:T(8,128)(2,1)} %refs_1_.1, bf16[4096,128]{1,0:T(8,128)(2,1)} %refs_2_.1, bf16[4096,128]{1,0:T(8,128)(2,1)} %refs_3_.1, bf16[64,4096]{1,0:T(8,128)(2,1)} %bitcast.3, s32[10,2,16]{2,1,0:T(2,128)} %refs_5_.1, bf16[8,32]{1,0:T(8,128)(2,1)} %bitcast.4, ...), custom_call_target="tpu_custom_call" | custom-call | tf_op jit(solution)/shard_map/layer/pallas_call | solution.py:861
  46.2 1.1 %copy.12 = bf16[160,4096]{1,0:T(8,128)(2,1)} copy(bf16[160,4096]{1,0:T(8,128)(2,1)S(1)} %layer.1) | data formatting | bytes 2621440

commit v5 on v4

--- a/solution.py
+++ b/solution.py
@@ -69,7 +69,7 @@
 
 
 class Travel:
-    SPLIT = ((0, 2), (2, 1), (3, 2))
+    SPLIT = ((0, 1), (1, 2), (3, 1), (4, 1))
 
     def __init__(self, k):
         tp, me = lax.axis_index("tp"), lax.axis_index("kv")
@@ -100,7 +100,7 @@
 
     def x(self, j):
         k = self.k
-        quarter, piece = (self.own, j) if j < 3 else (self.last, 2)
+        quarter, piece = (self.own, j) if j < 4 else (self.last, 3)
         return self.copy(
             k.ow_hbm.at[:, self.cols(quarter, piece, self.first)], k.wfar.at[1, :, self.cols(quarter, piece)],
             k.wx_s, k.wx_r.at[j], self.across,
@@ -124,6 +124,9 @@
 
     def g(self, j, arrival=False):
         return self.pass_on(self.last if arrival else self.by_second, j, (self.k.wg_s, self.k.wg_r), j, self.first_of)
+
+    def h(self, arrival=False):
+        return self.pass_on(self.last if arrival else self.by_first, 2, (self.k.wh_s, self.k.wh_r), 0, self.second_of)
 
     def d(self, q, j):
         k = self.k
@@ -133,21 +136,23 @@
         )
 
     def start(self):
-        for j in range(4):
+        for j in range(5):
             self.x(j).start()
         self.p().start()
 
     def relay_x(self, j):
         self.x(j).wait_recv()
-        if j < 3:
+        if j < 4:
             self.z(j).start()
             self.y(j).start()
             self.d(0, j).start()
         else:
-            self.d(3, 2).start()
+            self.d(3, 3).start()
 
     def relay_y(self, j):
         self.y(j, True).wait_recv()
+        if j == 2:
+            self.h().start()
         self.d(1, j).start()
 
     def relay_z(self, j):
@@ -156,6 +161,10 @@
             self.g(j).start()
         self.d(2, j).start()
 
+    def relay_h(self):
+        self.h(True).wait_recv()
+        self.d(3, 2).start()
+
     def relay_g(self, j):
         self.g(j, True).wait_recv()
         self.d(3, j).start()
@@ -171,7 +180,7 @@
     def sent(self):
         k, unit = self.k, self.columns // 20
         self.p().wait_send()
-        for sem, size in ((k.wx_s, 7), (k.wy_s, 5), (k.wz_s, 5), (k.wg_s, 3), (k.wd_s, 20)):
+        for sem, size in ((k.wx_s, 6), (k.wy_s, 5), (k.wz_s, 5), (k.wg_s, 3), (k.wh_s, 1), (k.wd_s, 20)):
             all_sent(k.wfar.at[1, :, pl.ds(0, size * unit)], sem)
 
 
@@ -369,8 +378,8 @@
         req_local(i).start()
     for i in range(n - 1, len(first), -1):
         answer(i)
+    travel.relay_x(0)
     lax.fori_loop(1, chunks, q_step, 0)
-    travel.relay_x(0)
     wide_low = lax.broadcasted_iota(jnp.int32, k.gacc.shape, 1) < half_gates
     gates = jax.nn.sigmoid(k.gacc[...])
     gates_hi = gates.astype(BF16).astype(F32)
@@ -606,6 +615,7 @@
     for c in ow_loads:
         c.wait()
     travel.relay_x(2)
+    travel.relay_x(3)
     blocks_done()
 
     def d_copy(j):
@@ -673,12 +683,10 @@
             x_copy(2 * i + h).start()
 
     relays = {
-        1: ((travel.relay_x, 3), (travel.relay_y, 0)),
-        2: ((travel.relay_y, 1),),
+        1: ((travel.relay_x, 4),),
+        2: ((travel.relay_y, 0), (travel.relay_y, 1)),
         3: ((travel.relay_z, 0),),
-        4: ((travel.relay_z, 1), (travel.relay_y, 2)),
-        8: ((travel.relay_g, 0), (travel.relay_z, 2)),
-        9: ((travel.relay_g, 1),),
+        4: ((travel.relay_y, 2), (travel.relay_y, 3)),
     }
     far_scores(n, G, k, block(0), 0)
     for i in range(nb):
@@ -702,6 +710,7 @@
         device_id={"tp": partner}, device_id_type=MESH,
     )
     p_copy.start()
+    travel.relay_z(1)
 
     def own_step(j, carry):
         w = ow[:, pl.ds(pl.multiple_of(j * cw, cw), cw)]
@@ -717,15 +726,18 @@
 
     p_copy.wait_recv()
     all_sent(k.att_in.at[pl.ds(1, 2)], k.a_r)
-    for q in range(4):
+    travel.p().wait_recv()
+
+    def wide(q):
         travel.arrived(q)
-        if q == 0:
-            travel.p().wait_recv()
         cols, out_cols = travel.quarter(q), travel.quarter(q, travel.first)
         o = jnp.dot(att[ours_at, :], ow[:, out_cols], preferred_element_type=F32)
         for slot in range(3):
             o = o + jnp.dot(k.att_in[slot], k.wfar[slot, :, cols], preferred_element_type=F32)
         k.out[:, out_cols] = o.astype(BF16)
+
+    wide(0)
+    wide(1)
     all_sent(k.drecv, k.d_r)
     all_sent(k.dsend, k.d_s)
 
@@ -736,6 +748,13 @@
 
     lax.fori_loop(0, chunks, base_step, 0)
 
+    travel.relay_g(0)
+    travel.relay_z(2)
+    travel.relay_z(3)
+    travel.relay_g(1)
+    travel.relay_h()
+    wide(2)
+    wide(3)
     all_sent(k.xrecv, k.x_r)
 
     def last_step(s, carry):
@@ -854,9 +873,9 @@
         "sum_s": dma((n,)), "sum_r": dma((n,)),
         "d_s": dma, "d_r": dma, "e_s": dma, "e_r": dma((half,)), "x_s": dma, "x_r": dma,
         "a_s": dma, "a_r": dma, "p_s": dma, "p_r": dma,
-        "wx_s": dma, "wx_r": dma((4,)), "wp_s": dma, "wp_r": dma,
-        "wy_s": dma, "wy_r": dma((3,)), "wz_s": dma, "wz_r": dma((3,)),
-        "wg_s": dma, "wg_r": dma((2,)), "wd_s": dma, "wd_r": dma((4,)),
+        "wx_s": dma, "wx_r": dma((5,)), "wp_s": dma, "wp_r": dma,
+        "wy_s": dma, "wy_r": dma((4,)), "wz_s": dma, "wz_r": dma((4,)),
+        "wh_s": dma, "wh_r": dma((1,)), "wg_s": dma, "wg_r": dma((2,)), "wd_s": dma, "wd_r": dma((4,)),
     }
     return pl.pallas_call(
         functools.partial(layer_kernel, n, G, R, nb, kc, cw, inputs + ["out"] + list(scratch)),

time: 47.6 us -> 46 us (0.966); the launches traced: 47.3 us -> 45.2 us
  Pallas kernels: 46.2 us -> 44.1 us
    pallas_call x1, Pallas kernels: 46.2 us -> 44.1 us  [local(): pl.pallas_call(functools.partial(layer_kernel, n, G, R, nb, kc, cw, input...]
where the time goes in v5:
time: 46 us; the launch traced here: 45.2 us
  Pallas kernels  44.1 us (96%)
  local copies, waits for them, and re-layouts  1.06 us (2%)
    pallas_call x1, Pallas kernels, local(): pl.pallas_call(functools.partial(layer_kernel, n, G, R, nb, kc, cw, input...  44.1 us
    unnamed x1, local copies, waits for them, and re-layouts  1.06 us

profile of v5, /device:TPU:1, one launch (start us, length us, event | category | flops | bytes accessed | tf_op | source)
XLA Modules:
  0.0 45.2 jit_solution(493180671560620410)
XLA Ops:
  0.0 44.1 %layer.1 = bf16[160,4096]{1,0:T(8,128)(2,1)S(1)} custom-call(bf16[640,4096]{1,0:T(8,128)(2,1)} %refs_0_.1, bf16[4096,512]{1,0:T(8,128)(2,1)} %refs_1_.1, bf16[4096,128]{1,0:T(8,128)(2,1)} %refs_2_.1, bf16[4096,128]{1,0:T(8,128)(2,1)} %refs_3_.1, bf16[64,4096]{1,0:T(8,128)(2,1)} %bitcast.3, s32[10,2,16]{2,1,0:T(2,128)} %refs_5_.1, bf16[8,32]{1,0:T(8,128)(2,1)} %bitcast.4, ...), custom_call_target="tpu_custom_call" | custom-call | tf_op jit(solution)/shard_map/layer/pallas_call | solution.py:880
  44.1 1.1 %copy.12 = bf16[160,4096]{1,0:T(8,128)(2,1)} copy(bf16[160,4096]{1,0:T(8,128)(2,1)S(1)} %layer.1) | data formatting | bytes 2621440
